TPU v7x, 32 devices: a whole 2x2x4 slice. The times are simulated.
32 devices in a mesh: rep: 2 (over x), fs: 8 (over z, y), tp: 2 (over core).
Axes of the slice: x: 2, y: 2, z: 4, core: 2. Of those that a mesh axis runs over, the one named last changes fastest.
Arguments:
- tokens: bfloat16 [16, 512, 2048], P(('rep', 'fs')), may hold values from -6 to 6
- gain_mix_pre: float32 [2048], P('fs'), may hold values from 0.1 to 1.9
- gain_mix_post: float32 [2048], P('fs'), may hold values from 0.1 to 1.9
- gain_mlp_pre: float32 [2048], P('fs'), may hold values from 0.1 to 1.9
- gain_mlp_post: float32 [2048], P('fs'), may hold values from 0.1 to 1.9
- x_weight: float32 [2048, 2048], P('fs', 'tp'), may hold values from -0.125 to 0.125
- gate_weight: float32 [2048, 2048], P('fs', 'tp'), may hold values from -0.125 to 0.125
- x_scale: float32 [2048], P('tp'), may hold values from 0.5 to 2
- gate_scale: float32 [2048], P('tp'), may hold values from 0.5 to 2
- conv_weight: float32 [4, 2048], P(None, 'tp'), may hold values from -3 to 3
- recur_map: bfloat16 [2048, 32], P('tp'), may hold values from -1 to 1
- input_map: bfloat16 [2048, 32], P('tp'), may hold values from -1 to 1
- decay_param: float32 [2048], P('tp'), may hold values from 3.9 to 10
- out_weight: float32 [2048, 2048], P('tp', 'fs'), may hold values from -0.125 to 0.125
- out_scale: float32 [2048], P('fs'), may hold values from 0.5 to 2
- up_weight: float32 [2048, 6144], P('fs', 'tp'), may hold values from -0.125 to 0.125
- up_scale: float32 [6144], P('tp'), may hold values from 0.5 to 2
- down_weight: float32 [6144, 2048], P('tp', 'fs'), may hold values from -0.078125 to 0.078125
- down_scale: float32 [2048], P('fs'), may hold values from 0.5 to 2
Outputs:
- layer_out: bfloat16 [16, 512, 2048], P(('rep', 'fs'), 'tp')
All inputs are finite; a program needn't handle non-finite values.
Results may differ from a plain program's by a relative error of at most 0.025.
Values may be sent and summed in bfloat16 or wider, within the bound.
A program may use at most 128 MiB of HBM per device.

v0:
```python
import functools

import jax
import jax.numpy as jnp
from jax import lax
from jax.experimental import pallas as pl
from jax.experimental.pallas import tpu as pltpu
from jax.sharding import PartitionSpec as P

BLOCK = 32
LANES = 128
EPSILON = 1e-06
DECAY_SCALE = 8.0
F32 = jnp.float32
BF16 = jnp.bfloat16


def unit_rows(values):
    return values * lax.rsqrt(jnp.mean(values * values, axis=-1, keepdims=True) + EPSILON)


def shifted(values, distance, fill):
    head = jnp.full((distance, values.shape[1]), fill, values.dtype)
    return jnp.concatenate([head, values[: values.shape[0] - distance]], axis=0)


def mixer_kernel(x_ref, gate_ref, taps_ref, recur_ref, input_ref, rate_ref, mixed_ref):
    length = x_ref.shape[0]
    x_branch = x_ref[...].astype(F32)
    taps = taps_ref.shape[0]
    total = taps_ref[taps - 1 : taps, :] * x_branch
    for tap in range(taps - 1):
        total += taps_ref[tap : tap + 1, :] * shifted(x_branch, taps - 1 - tap, 0.0)
    conv = total.astype(BF16)
    recur = jax.nn.sigmoid(jnp.dot(conv, recur_ref[...], preferred_element_type=F32))
    gate_in = jax.nn.sigmoid(jnp.dot(conv, input_ref[...], preferred_element_type=F32))
    log_decay = recur * rate_ref[0:1, :]
    decay = jnp.exp(log_decay)
    z = -2.0 * log_decay
    series = z * (1.0 - z * (1 / 2) * (1.0 - z * (1 / 3) * (1.0 - z * (1 / 4) * (1.0 - z * (1 / 5)))))
    power = jnp.where(z < 0.1, series, 1.0 - decay * decay)
    state = jnp.sqrt(power) * gate_in * conv.astype(F32)
    distance = 1
    while distance < length:
        state = state + decay * shifted(state, distance, 0.0)
        decay = decay * shifted(decay, distance, 1.0)
        distance *= 2
    mixed_ref[...] = (state * jax.nn.gelu(gate_ref[...].astype(F32))).astype(BF16)


def mixer(branches, taps, recur_dense, input_dense, rate, sequences):
    rows, width = branches.shape[0], branches.shape[1] // 2
    length = rows // sequences
    groups = width // LANES
    return pl.pallas_call(
        mixer_kernel,
        grid=(sequences, groups),
        in_specs=[
            pl.BlockSpec((length, LANES), lambda s, g: (s, g)),
            pl.BlockSpec((length, LANES), lambda s, g: (s, g + groups)),
            pl.BlockSpec((taps.shape[0], LANES), lambda s, g: (0, g)),
            pl.BlockSpec((LANES, LANES), lambda s, g: (g, 0)),
            pl.BlockSpec((LANES, LANES), lambda s, g: (g, 0)),
            pl.BlockSpec((1, LANES), lambda s, g: (0, g)),
        ],
        out_specs=pl.BlockSpec((length, LANES), lambda s, g: (s, g)),
        out_shape=jax.ShapeDtypeStruct((rows, width), BF16),
        cost_estimate=pl.CostEstimate(
            flops=rows * width * 100, bytes_accessed=rows * width * 6, transcendentals=rows * width * 4
        ),
        name="mixer",
    )(branches, branches, taps, recur_dense, input_dense, rate)


MESH_IDS = pl.DeviceIdType.MESH


def greet(peers):
    barrier = pltpu.get_barrier_semaphore()
    for peer in peers:
        pl.semaphore_signal(barrier, inc=1, device_id=peer, device_id_type=MESH_IDS)
    pl.semaphore_wait(barrier, len(peers))


def push(source, target, sent, landed, peer):
    return pltpu.make_async_remote_copy(
        src_ref=source, dst_ref=target, send_sem=sent, recv_sem=landed,
        device_id=peer, device_id_type=MESH_IDS,
    )


def others(axis, count):
    me = lax.axis_index(axis)
    return [lax.rem(me + step, count) for step in range(1, count)]


def row_block(ref, index, rows):
    return ref.at[pl.ds(pl.multiple_of(index * rows, rows), rows)]


def team_gather_kernel(reps, tps, x_ref, out_ref, own_sem, sent, landed):
    rep, core = lax.axis_index("rep"), lax.axis_index("tp")
    rows = x_ref.shape[0]
    rep_peers, tp_peers = others("rep", reps), others("tp", tps)
    greet([{"rep": peer} for peer in rep_peers] + [{"tp": peer} for peer in tp_peers])
    mine = row_block(out_ref, rep * tps + core, rows)
    flights = []
    for step, peer in enumerate(rep_peers):
        copy = push(x_ref, mine, sent.at[step + 1, 0], landed.at[step + 1, 0], {"rep": peer})
        copy.start()
        flights.append(copy)
    own = pltpu.make_async_copy(x_ref, mine, own_sem)
    own.start()
    local = []
    for slot, peer in enumerate(tp_peers):
        copy = push(x_ref, mine, sent.at[0, slot + 1], landed.at[0, slot + 1], {"tp": peer})
        copy.start()
        local.append(copy)
    for step in range(1, reps):
        flights[step - 1].wait_recv()
        source = lax.rem(rep + reps - step, reps)
        block = row_block(out_ref, source * tps + core, rows)
        for slot, peer in enumerate(tp_peers):
            copy = push(block, block, sent.at[step, slot + 1], landed.at[step, slot + 1], {"tp": peer})
            copy.start()
            local.append(copy)
    for copy in flights:
        copy.wait_send()
    for copy in local:
        copy.wait()
    own.wait()


def team_gather(values):
    reps, tps = lax.axis_size("rep"), lax.axis_size("tp")
    rows, width = values.shape
    return pl.pallas_call(
        functools.partial(team_gather_kernel, reps, tps),
        out_shape=jax.ShapeDtypeStruct((rows * reps * tps, width), values.dtype),
        in_specs=[pl.BlockSpec(memory_space=pltpu.VMEM)],
        out_specs=pl.BlockSpec(memory_space=pltpu.VMEM),
        scratch_shapes=[
            pltpu.SemaphoreType.DMA,
            pltpu.SemaphoreType.DMA((reps, tps)),
            pltpu.SemaphoreType.DMA((reps, tps)),
        ],
        compiler_params=pltpu.CompilerParams(collective_id=0, has_side_effects=True),
        cost_estimate=pl.CostEstimate(flops=0, bytes_accessed=80_000_000, transcendentals=0),
        name="team_gather",
    )(values)


def team_sum_kernel(reps, tps, part_ref, out_ref, got, stage, last, sent, landed, sent_far, landed_far):
    rep, core = lax.axis_index("rep"), lax.axis_index("tp")
    rows = out_ref.shape[0]
    step_rows = 16
    rep_peers, tp_peers = others("rep", reps), others("tp", tps)
    greet([{"rep": peer} for peer in rep_peers] + [{"tp": peer} for peer in tp_peers])
    near = []
    for slot, peer in enumerate(tp_peers):
        for group in range(reps):
            copy = push(
                row_block(part_ref, group * tps + peer, rows), got.at[slot, group],
                sent.at[slot, group], landed.at[slot, group], {"tp": peer},
            )
            copy.start()
            near.append(copy)
    for copy in near:
        copy.wait()

    def total(group, start):
        base = pl.multiple_of((group * tps + core) * rows + start, step_rows)
        value = part_ref[pl.ds(base, step_rows)].astype(F32)
        for slot in range(tps - 1):
            value += got[slot, group, pl.ds(start, step_rows)].astype(F32)
        return value

    far = []
    for step, peer in enumerate(rep_peers):

        def fill(index, carry):
            start = pl.multiple_of(index * step_rows, step_rows)
            stage[step, pl.ds(start, step_rows)] = total(peer, start).astype(BF16)
            return carry

        lax.fori_loop(0, rows // step_rows, fill, 0)
        copy = push(stage.at[step], last.at[step], sent_far.at[step], landed_far.at[step], {"rep": peer})
        copy.start()
        far.append(copy)
    for copy in far:
        copy.wait()

    def finish(index, carry):
        start = pl.multiple_of(index * step_rows, step_rows)
        value = total(rep, start)
        for step in range(reps - 1):
            value += last[step, pl.ds(start, step_rows)].astype(F32)
        out_ref[pl.ds(start, step_rows)] = value
        return carry

    lax.fori_loop(0, rows // step_rows, finish, 0)


def team_sum(parts):
    reps, tps = lax.axis_size("rep"), lax.axis_size("tp")
    rows, width = parts.shape[0] // (reps * tps), parts.shape[1]
    return pl.pallas_call(
        functools.partial(team_sum_kernel, reps, tps),
        out_shape=jax.ShapeDtypeStruct((rows, width), F32),
        in_specs=[pl.BlockSpec(memory_space=pltpu.VMEM)],
        out_specs=pl.BlockSpec(memory_space=pltpu.VMEM),
        scratch_shapes=[
            pltpu.VMEM((tps - 1, reps, rows, width), BF16),
            pltpu.VMEM((reps - 1, rows, width), BF16),
            pltpu.VMEM((reps - 1, rows, width), BF16),
            pltpu.SemaphoreType.DMA((tps - 1, reps)),
            pltpu.SemaphoreType.DMA((tps - 1, reps)),
            pltpu.SemaphoreType.DMA((reps - 1,)),
            pltpu.SemaphoreType.DMA((reps - 1,)),
        ],
        compiler_params=pltpu.CompilerParams(collective_id=1, has_side_effects=True),
        cost_estimate=pl.CostEstimate(flops=0, bytes_accessed=80_000_000, transcendentals=0),
        name="team_sum",
    )(parts)


def shard_gather_kernel(shards, x_ref, out_ref, own_sem, sent, landed, sent_pass, landed_pass):
    me = lax.axis_index("fs")
    rows = x_ref.shape[0]
    pairs = shards // 2
    pair, parity = me // 2, lax.rem(me, 2)
    partner = {"fs": pair * 2 + 1 - parity}
    peers = [{"fs": lax.rem(pair + step, pairs) * 2 + parity} for step in range(1, pairs)]
    greet([partner] + peers)
    mine = row_block(out_ref, me, rows)
    passed = [push(x_ref, mine, sent_pass.at[0], landed_pass.at[0], partner)]
    passed[0].start()
    direct = []
    for step, peer in enumerate(peers):
        copy = push(x_ref, mine, sent.at[step], landed.at[step], peer)
        copy.start()
        direct.append(copy)
    own = pltpu.make_async_copy(x_ref, mine, own_sem)
    own.start()
    for step in range(1, pairs):
        direct[step - 1].wait_recv()
        block = row_block(out_ref, lax.rem(pair + pairs - step, pairs) * 2 + parity, rows)
        copy = push(block, block, sent_pass.at[step], landed_pass.at[step], partner)
        copy.start()
        passed.append(copy)
    for copy in direct:
        copy.wait_send()
    for copy in passed:
        copy.wait()
    own.wait()


def shard_gather(values, collective_id):
    shards = lax.axis_size("fs")
    rows, width = values.shape
    return pl.pallas_call(
        functools.partial(shard_gather_kernel, shards),
        out_shape=jax.ShapeDtypeStruct((rows * shards, width), values.dtype),
        in_specs=[pl.BlockSpec(memory_space=pltpu.VMEM)],
        out_specs=pl.BlockSpec(memory_space=pltpu.VMEM),
        scratch_shapes=[
            pltpu.SemaphoreType.DMA,
            pltpu.SemaphoreType.DMA((shards // 2,)),
            pltpu.SemaphoreType.DMA((shards // 2,)),
            pltpu.SemaphoreType.DMA((shards // 2,)),
            pltpu.SemaphoreType.DMA((shards // 2,)),
        ],
        compiler_params=pltpu.CompilerParams(collective_id=collective_id, has_side_effects=True),
        cost_estimate=pl.CostEstimate(flops=0, bytes_accessed=200_000_000, transcendentals=0),
        name="shard_gather",
    )(values)


def on_device(
    tokens, gain_mix_pre, gain_mix_post, gain_mlp_pre, gain_mlp_post,
    x_weight, gate_weight, x_scale, gate_scale, conv_weight, recur_map, input_map,
    decay_param, out_weight, out_scale, up_weight, up_scale, down_weight, down_scale,
):
    reps = lax.axis_size("rep")
    rep = lax.axis_index("rep")

    def part(values, axis):
        size = values.shape[axis] // reps
        return lax.dynamic_slice_in_dim(values, rep * size, size, axis)

    length = tokens.shape[1]
    share_rows = length // lax.axis_size("tp")
    offset_row = lax.axis_index("tp") * share_rows
    resid_share = lax.dynamic_slice_in_dim(tokens[0], offset_row, share_rows, 0).astype(F32)
    normed_share = unit_rows(resid_share).astype(BF16)

    pre = gain_mix_pre[:, None]
    branch_rows = jnp.concatenate(
        [(part(x_weight, 1) * pre).astype(BF16), (part(gate_weight, 1) * pre).astype(BF16)], axis=1
    )
    branch_rows, out_weight = lax.optimization_barrier((branch_rows, out_weight))
    branch_full = lax.all_gather(branch_rows, "fs", axis=0, tiled=True)
    post = jnp.stack([gain_mix_post, gain_mlp_post])
    post_high = post.astype(BF16)
    post_low = (post - post_high.astype(F32)).astype(BF16)
    pad_rows = jnp.zeros((12, post.shape[1]), BF16)
    out_cols = jnp.concatenate(
        [(part(out_weight, 0) * out_scale).astype(BF16), post_high, post_low, pad_rows], axis=0
    )
    out_cols, down_weight = lax.optimization_barrier((out_cols, down_weight))
    out_all = lax.all_gather(out_cols, "fs", axis=1, tiled=True)
    down_full = lax.all_gather((part(down_weight, 0) * down_scale).astype(BF16), "fs", axis=1, tiled=True)
    up_rows = (part(up_weight, 1) * gain_mlp_pre[:, None]).astype(BF16)
    normed = team_gather(normed_share)
    normed, up_rows = lax.optimization_barrier((normed, up_rows))
    up_full = shard_gather(up_rows, 2)
    normed, up_full = lax.optimization_barrier((normed, up_full))

    scales = jnp.concatenate([part(x_scale, 0), part(gate_scale, 0)])
    branches = (jnp.dot(normed, branch_full, preferred_element_type=F32) * scales).astype(BF16)
    width = branches.shape[1] // 2

    def dense(block_map):
        rows = lax.broadcasted_iota(jnp.int32, (width, LANES), 0)
        columns = lax.broadcasted_iota(jnp.int32, (width, LANES), 1)
        spread = jnp.tile(part(block_map, 0), (1, LANES // BLOCK))
        return jnp.where(rows % LANES // BLOCK == columns // BLOCK, spread, 0).astype(BF16)

    rate = -DECAY_SCALE * jax.nn.softplus(-part(decay_param, 0))
    mixed = mixer(
        branches, part(conv_weight, 1), dense(recur_map), dense(input_map), rate[None], reps
    )
    out_full = out_all[:width]
    gains = out_all[width : width + 2].astype(F32) + out_all[width + 2 : width + 4].astype(F32)
    mix_share = team_sum(jnp.dot(mixed, out_full, preferred_element_type=F32).astype(BF16))
    hidden_state = (resid_share + unit_rows(mix_share) * gains[0]).astype(BF16)
    mlp_input = team_gather(unit_rows(hidden_state.astype(F32)).astype(BF16))
    up_proj = jnp.dot(mlp_input, up_full, preferred_element_type=F32)
    activated = jnp.square(jax.nn.relu(up_proj * part(up_scale, 0))).astype(BF16)
    mlp_share = team_sum(jnp.dot(activated, down_full, preferred_element_type=F32).astype(BF16))
    return (hidden_state.astype(F32) + unit_rows(mlp_share) * gains[1]).astype(BF16)[None]


def solution(mesh):
    in_specs = (
        P(("rep", "fs"), None, None),
        P("fs"), P("fs"), P("fs"), P("fs"),
        P("fs", "tp"), P("fs", "tp"),
        P("tp"), P("tp"),
        P(None, "tp"), P("tp", None), P("tp", None), P("tp"),
        P("tp", "fs"), P("fs"),
        P("fs", "tp"), P("tp"),
        P("tp", "fs"), P("fs"),
    )
    out_specs = P(("rep", "fs"), "tp", None)
    return jax.shard_map(
        on_device, mesh=mesh, in_specs=in_specs, out_specs=out_specs, check_vma=False
    )
```

profile of v0, /device:TPU:0, one launch (start us, length us, event | category | flops | bytes accessed | tf_op | source)
XLA Modules:
  0.0 379.0 jit_solution(17023048875819067327)
XLA Ops:
  6.6 0.8 fusion.19
  8.1 1.3 multiply_convert_fusion.6
  9.4 0.9 pad_maximum_fusion
  10.4 0.9 maximum_maximum_fusion
  12.1 2.5 multiply_convert_fusion.2
  15.0 1.2 fusion.4.x_ref
  16.2 32.4 %team_gather.2 = bf16[1024,2048]{1,0:T(8,128)(2,1)} custom-call(bf16[256,2048]{1,0:T(8,128)(2,1)} %fusion.4.x_ref), custom_call_target="tpu_custom_call" | custom-call | bytes 80000000 | tf_op jit(solution)/shard_map/team_gather/pallas_call | solution.py:137
  48.5 2.5 multiply_convert_fusion.3.x_ref
  51.0 103.3 %shard_gather.1 = bf16[2048,1536]{1,0:T(8,128)(2,1)} custom-call(bf16[256,1536]{1,0:T(8,128)(2,1)} %multiply_convert_fusion.3.x_ref), custom_call_target="tpu_custom_call" | custom-call | bytes 200000000 | tf_op jit(solution)/shard_map/shard_gather/pallas_call | solution.py:261
  156.3 1.0 broadcast_select_fusion
  157.3 0.8 convert_add_fusion.2
  158.1 41.6 %all-gather.4.cloned.1.call-done = bf16[2048,1024]{1,0:T(8,128)(2,1)} async-done(((bf16[256,1024]{1,0:T(8,128)(2,1)}), bf16[2048,1024]{1,0:T(8,128)(2,1)}) %all-gather.4.cloned.1.call-update) | async-done | bytes 4194320 | tf_op jit(solution)/shard_map/all_gather | solution.py:302
  199.8 9.3 %multiply_convert_fusion.1.x_ref.gate_ref = bf16[1024,1024]{1,0:T(8,128)(2,1)} fusion(bf16[1024,2048]{1,0:T(8,128)(2,1)} %team_gather.2, bf16[2048,1024]{1,0:T(8,128)(2,1)} %all-gather.4.cloned.1.call-done, f32[1024]{0:T(1024)S(1)} %pad_maximum_fusion.1), kind=kOutput, calls=%fused_computation.1 | convolution fusion | flops 4297064448 | bytes 10489856 | tf_op jit(solution)/shard_map/dot_general | solution.py:320
  209.1 9.6 %mixer.1 = bf16[1024,512]{1,0:T(8,128)(2,1)} custom-call(bf16[1024,1024]{1,0:T(8,128)(2,1)} %multiply_convert_fusion.1.x_ref.gate_ref, bf16[1024,1024]{1,0:T(8,128)(2,1)} %multiply_convert_fusion.1.x_ref.gate_ref, f32[4,512]{1,0:T(4,128)} %constant_dynamic-slice_fusion.2.taps_ref, bf16[512,128]{1,0:T(8,128)(2,1)} %get-tuple-element.26.recur_ref, ...), custom_call_target="tpu_custom_call" | custom-call | flops 52428800 | bytes 3145728 | tf_op jit(solution)/shard_map/mixer/pallas_call | solution.py:55
  218.6 6.2 %convolution_convert_fusion.1.part_ref = bf16[1024,2048]{1,0:T(8,128)(2,1)} fusion(bf16[1024,512]{1,0:T(8,128)(2,1)} %mixer.1, bf16[528,2048]{1,0:T(8,128)(2,1)} %all-gather.6.cloned.1.call-done), kind=kOutput, calls=%fused_computation.3 | convolution fusion | flops 2149580800 | bytes 7340032 | tf_op jit(solution)/shard_map/dot_general | solution.py:335
  224.8 34.0 %team_sum.2 = f32[256,2048]{1,0:T(8,128)} custom-call(bf16[1024,2048]{1,0:T(8,128)(2,1)} %convolution_convert_fusion.1.part_ref), custom_call_target="tpu_custom_call" | custom-call | bytes 80000000 | tf_op jit(solution)/shard_map/team_sum/pallas_call | solution.py:207
  258.9 2.0 multiply_reduce_fusion.1
  261.9 1.2 fusion.1.x_ref
  263.1 30.9 %team_gather.3 = bf16[1024,2048]{1,0:T(8,128)(2,1)} custom-call(bf16[256,2048]{1,0:T(8,128)(2,1)} %fusion.1.x_ref), custom_call_target="tpu_custom_call" | custom-call | bytes 80000000 | tf_op jit(solution)/shard_map/team_gather/pallas_call | solution.py:137
  293.9 21.2 %all-gather.8.cloned.1.call-done = bf16[1536,2048]{1,0:T(8,128)(2,1)} async-done(((bf16[1536,256]{1,0:T(8,128)(2,1)}), bf16[1536,2048]{1,0:T(8,128)(2,1)}) %all-gather.8.cloned.1.call-update) | async-done | bytes 6291472 | tf_op jit(solution)/shard_map/all_gather | solution.py:312
  315.1 19.9 %convolution_convert_fusion.part_ref = bf16[1024,2048]{1,0:T(8,128)(2,1)} fusion(bf16[1536,2048]{1,0:T(8,128)(2,1)} %all-gather.8.cloned.1.call-done, bf16[1024,2048]{1,0:T(8,128)(2,1)} %team_gather.3, bf16[2048,1536]{1,0:T(8,128)(2,1)} %shard_gather.1, f32[1536]{0:T(1024)S(1)} %dynamic_slice.50), kind=kOutput, calls=%fused_computation.2 | convolution fusion | flops 12893290496 | bytes 20977664 | tf_op jit(solution)/shard_map/dot_general | solution.py:340
  335.0 33.9 %team_sum.3 = f32[256,2048]{1,0:T(8,128)} custom-call(bf16[1024,2048]{1,0:T(8,128)(2,1)} %convolution_convert_fusion.part_ref), custom_call_target="tpu_custom_call" | custom-call | bytes 80000000 | tf_op jit(solution)/shard_map/team_sum/pallas_call | solution.py:207
  368.9 2.0 multiply_reduce_fusion
  371.1 1.3 fusion.7
  (61 shorter events, 5.0 us)
Async XLA Ops:
  6.5 149.1 %copy-start = (f32[4,1024]{1,0:T(4,128)S(1)}, f32[4,1024]{1,0:T(4,128)}, u32[]{:S(2)}) copy-start(f32[4,1024]{1,0:T(4,128)} %param.28) | copy-start | bytes 49156
  6.5 3.7 copy-start.4
  6.5 3.7 copy-start.8
  6.5 150.7 %all-gather.6.cloned.1.call-start = ((), (), s32[]{:S(2)}) async-start(), calls=%async_computation.1 | async-start | bytes 2433024 | tf_op jit(solution)/shard_map/all_gather | solution.py:311
  8.1 4.1 %copy-start.9 = (f32[256]{0:T(256)S(1)}, f32[256]{0:T(256)}, u32[]{:S(2)}) copy-start(f32[256]{0:T(256)} %param.37) | copy-start | bytes 3076
  10.4 4.2 %copy-start.3 = (bf16[1,512,2048]{2,1,0:T(8,128)(2,1)S(1)}, bf16[1,512,2048]{2,1,0:T(8,128)(2,1)}, u32[]{:S(2)}) copy-start(bf16[1,512,2048]{2,1,0:T(8,128)(2,1)} %param.19) | copy-start | bytes 6291460
  11.3 188.5 %all-gather.4.cloned.1.call-start = ((), (), s32[]{:S(2)}) async-start(), calls=%async_computation | async-start | bytes 4718592 | tf_op jit(solution)/shard_map/all_gather | solution.py:302
  12.1 303.1 %all-gather.8.cloned.1.call-start = ((), (), s32[]{:S(2)}) async-start(), calls=%async_computation.2 | async-start | bytes 7077888 | tf_op jit(solution)/shard_map/all_gather | solution.py:312
  16.2 32.4 %copy-start.10 = (f32[256]{0:T(256)S(1)}, f32[256]{0:T(256)}, u32[]{:S(2)}) copy-start(f32[256]{0:T(256)} %param.22) | copy-start | bytes 3076
  51.0 103.4 %copy-start.11 = (f32[1024]{0:T(1024)S(1)}, f32[1024]{0:T(1024)}, u32[]{:S(2)}) copy-start(f32[1024]{0:T(1024)} %param.26) | copy-start | bytes 12292
  51.0 103.5 %copy-start.12 = (f32[1024]{0:T(1024)S(1)}, f32[1024]{0:T(1024)}, u32[]{:S(2)}) copy-start(f32[1024]{0:T(1024)} %param.27) | copy-start | bytes 12292
  51.0 103.5 %copy-start.5 = (bf16[1024,32]{0,1:T(8,128)(2,1)S(1)}, bf16[1024,32]{0,1:T(8,128)(2,1)}, u32[]{:S(2)}) copy-start(bf16[1024,32]{0,1:T(8,128)(2,1)} %param.30) | copy-start | bytes 196612
  51.0 103.5 %copy-start.6 = (bf16[1024,32]{0,1:T(8,128)(2,1)S(1)}, bf16[1024,32]{0,1:T(8,128)(2,1)}, u32[]{:S(2)}) copy-start(bf16[1024,32]{0,1:T(8,128)(2,1)} %param.29) | copy-start | bytes 196612
  51.0 103.8 %copy-start.7 = (f32[3072]{0:T(1024)S(1)}, f32[3072]{0:T(1024)}, u32[]{:S(2)}) copy-start(f32[3072]{0:T(1024)} %param.35) | copy-start | bytes 36868
  51.0 103.9 %copy-start.13 = (f32[1024]{0:T(1024)S(1)}, f32[1024]{0:T(1024)}, u32[]{:S(2)}) copy-start(f32[1024]{0:T(1024)} %param.31) | copy-start | bytes 12292
  258.8 2.4 copy-start.1
  368.9 2.2 copy-start.2
Sparse Core Ops, SparseCore 0:
  11.4 89.6 all-gather.5
  103.3 96.4 all-gather.3
  201.8 113.2 all-gather.7
where the time goes:
time: 380 us; the launch traced here: 379 us
  Pallas kernels  244 us (64%)
  waiting for transfers between devices  63.5 us (17%)
  matrix products  35.4 us (9%)
  other arithmetic  20.8 us (5%)
  between operations  13.4 us (4%)
    pallas_call x1, Pallas kernels, shard_gather(): pl.pallas_call(functools.partial(shard_gather_kernel, shards), out_shape=...  103 us
    pallas_call x2, Pallas kernels, team_sum(): pl.pallas_call(functools.partial(team_sum_kernel, reps, tps), out_shape=j...  67.9 us
    pallas_call x2, Pallas kernels, team_gather(): pl.pallas_call(functools.partial(team_gather_kernel, reps, tps), out_shap...  63.2 us
    all_gather x1, waiting for transfers between devices, on_device(): branch_full = lax.all_gather(branch_rows, 'fs', axis=0, tiled=True)  41.6 us
    all_gather x1, waiting for transfers between devices, on_device(): lax.all_gather((part(down_weight, 0) * down_scale).astype(BF16), 'fs', ax...  21.2 us
    dot_general x1, matrix products, on_device(): jnp.dot(activated, down_full, preferred_element_type=F32).astype(BF16)  19.9 us
    pallas_call x1, Pallas kernels, mixer(): pl.pallas_call(mixer_kernel, grid=(sequences, groups), in_specs=[pl.Block...  9.55 us
    dot_general x1, matrix products, on_device(): jnp.dot(normed, branch_full, preferred_element_type=F32) * scales  9.32 us
  transfers between devices with their start and end apart: 3, of which 2 were waited for; matrix products, arithmetic and copies ran while one was open for 8% of the time, Pallas kernels for 55%

commit v1 on v0

--- a/solution.py
+++ b/solution.py
@@ -341,6 +341,541 @@
     return (hidden_state.astype(F32) + unit_rows(mlp_share) * gains[1]).astype(BF16)[None]
 
 
+WEIGHTS = 4
+PIECE = 256
+
+
+def mixer_group(x_branch, gate, taps, recur_map, input_map, rate):
+    length, count = x_branch.shape[0], taps.shape[0]
+    total = taps[count - 1 : count, :] * x_branch
+    for tap in range(count - 1):
+        total += taps[tap : tap + 1, :] * shifted(x_branch, count - 1 - tap, 0.0)
+    conv = total.astype(BF16)
+    recur = jax.nn.sigmoid(jnp.dot(conv, recur_map, preferred_element_type=F32))
+    gate_in = jax.nn.sigmoid(jnp.dot(conv, input_map, preferred_element_type=F32))
+    log_decay = recur * rate
+    decay = jnp.exp(log_decay)
+    z = -2.0 * log_decay
+    series = z * (1.0 - z * (1 / 2) * (1.0 - z * (1 / 3) * (1.0 - z * (1 / 4) * (1.0 - z * (1 / 5)))))
+    power = jnp.where(z < 0.1, series, 1.0 - decay * decay)
+    state = jnp.sqrt(power) * gate_in * conv.astype(F32)
+    distance = 1
+    while distance < length:
+        state = state + decay * shifted(state, distance, 0.0)
+        decay = decay * shifted(decay, distance, 1.0)
+        distance *= 2
+    return (state * jax.nn.gelu(gate)).astype(BF16)
+
+
+def aligned(start, unit):
+    return pl.multiple_of(start, unit)
+
+
+def layer_kernel(
+    shards, tokens, gains, b_parts, o_parts, u_parts, d_parts, scales, up_scale, taps, recur_map, input_map, rate,
+    out, b_full, o_full, u_full, d_full, gains_full, tok_got, normed, branches, mixed, mlp_in, active, hidden,
+    give, got_near, keep, total, stage, got_far,
+    own_sem, y_sent, y_land, z_sent, z_land, zf_sent, x_sent, x_land, g_own, g_sent, g_land,
+    t_sent, t_land, n_sent, n_land, f_sent, f_land, m_sent, m_land, mn_sent, mn_land, mf_sent, mf_land,
+):
+    lines = shards // 2
+    others = lines - 1
+    rep, me, core = lax.axis_index("rep"), lax.axis_index("fs"), lax.axis_index("tp")
+    z, y = me // 2, lax.rem(me, 2)
+    x_peer, core_peer, y_peer = {"rep": 1 - rep}, {"tp": 1 - core}, {"fs": z * 2 + 1 - y}
+    upper = z // (lines // 2)
+    depth = z + upper * (lines - 1 - 2 * z)
+
+    def other(k):
+        place = k + (k + lines - depth) // lines
+        return place + upper * (lines - 1 - 2 * place)
+
+    greet(
+        [{"fs": lax.rem(me + step, shards)} for step in range(1, shards)] + [x_peer, core_peer]
+    )
+    parts = (b_parts, o_parts, u_parts, d_parts)
+    fulls = (b_full, o_full, u_full, d_full)
+
+    def half(w, slot, side):
+        rows = parts[w].shape[1]
+        return fulls[w].at[pl.ds(aligned(slot * rows + side * (rows // 2), 64), rows // 2)]
+
+    def whole(w, slot):
+        rows = parts[w].shape[1]
+        return fulls[w].at[pl.ds(aligned(slot * rows, 64), rows)]
+
+    def y_copy(w):
+        return push(parts[w].at[1 - y], whole(w, me), y_sent.at[w], y_land.at[w], y_peer)
+
+    def y_arrival(w):
+        block = whole(w, z * 2 + 1 - y)
+        return push(block, block, y_sent.at[w], y_land.at[w], y_peer)
+
+    def own_copy(w):
+        return pltpu.make_async_copy(parts[w].at[y], whole(w, me), own_sem.at[w])
+
+    def z_copy(w, kind, k):
+        slot = z * 2 + lax.rem(y + kind, 2)
+        target = half(w, slot, rep)
+        rows = parts[w].shape[1] // 2
+        source = parts[w].at[y, pl.ds(aligned(rep * rows, 64), rows)] if kind == 0 else target
+        return push(source, target, z_sent.at[w, kind, k], z_land.at[w, slot], {"fs": other(k) * 2 + y})
+
+    def start_z(w, kind):
+        for k in range(others - 1):
+            z_copy(w, kind, k).start()
+
+        @pl.when(depth > 0)
+        def _():
+            z_copy(w, kind, others - 1).start()
+
+    def item_slot(kind, k):
+        return other(k) * 2 + lax.rem(y + kind, 2)
+
+    def zf_copy(w, kind):
+        block = half(w, item_slot(kind, others - 1), rep)
+        ends = upper * (lines - 1)
+        return push(block, block, zf_sent.at[w, kind], z_land.at[w, item_slot(kind, others - 1)], {"fs": ends * 2 + y})
+
+    def x_copy(w, kind, k):
+        slot = item_slot(kind, k)
+        block = half(w, slot, rep)
+        return push(block, block, x_sent.at[w, kind, k], x_land.at[w, slot], x_peer)
+
+    def serve(w, kind, k):
+        slot = item_slot(kind, k)
+        block = half(w, slot, rep)
+        push(block, block, x_sent.at[w, kind, k], z_land.at[w, slot], x_peer).wait_recv()
+        x_copy(w, kind, k).start()
+
+        def onward():
+            zf_copy(w, kind).start()
+
+        if isinstance(k, int):
+            if k == others - 1:
+                pl.when(depth == 1)(onward)
+        else:
+            pl.when((k == others - 1) & (depth == 1))(onward)
+
+    def x_arrival(w, kind, k):
+        slot = item_slot(kind, k)
+        block = half(w, slot, 1 - rep)
+        push(block, block, x_sent.at[w, kind, k], x_land.at[w, slot], x_peer).wait_recv()
+
+    def all_x_arrivals(w):
+        def body(index, carry):
+            x_arrival(w, index // others, lax.rem(index, others))
+            return carry
+
+        lax.fori_loop(0, 2 * others, body, 0)
+
+    def serve_step(w, index, count=2 * others):
+        @pl.when((index >= 0) & (index < count))
+        def _():
+            serve(w, index // others, lax.rem(index, others))
+
+    seq = tokens.shape[0]
+    share = seq // 2
+    width = tokens.shape[1]
+    mine = pl.ds(aligned(core * share, 64), share)
+    t_near = push(tokens.at[mine], tok_got.at[mine], t_sent.at[0], t_land.at[0], y_peer)
+    t_pass = push(tok_got.at[mine], tok_got.at[mine], t_sent.at[1], t_land.at[1], core_peer)
+
+    y_copy(0).start()
+    start_z(0, 0)
+    t_near.start()
+    for w in range(1, WEIGHTS):
+        y_copy(w).start()
+    for w in range(WEIGHTS):
+        own_copy(w).start()
+    own_gains = pltpu.make_async_copy(gains, gains_full.at[me], g_own)
+    own_gains.start()
+
+    def gain_copy(step):
+        return push(gains, gains_full.at[me], g_sent.at[step - 1], g_land.at[me], {"fs": lax.rem(me + step, shards)})
+
+    for step in range(1, shards):
+        gain_copy(step).start()
+
+    rows = 16
+
+    def normalize(source, base):
+        def body(index, carry):
+            start = aligned(index * rows, rows)
+            values = source[pl.ds(start, rows), :].astype(F32)
+            normed[pl.ds(aligned(base + start, rows), rows), :] = unit_rows(values).astype(BF16)
+            return carry
+
+        lax.fori_loop(0, seq // rows, body, 0)
+
+    normalize(tokens, 0)
+    y_arrival(0).wait_recv()
+    start_z(0, 1)
+    start_z(1, 0)
+    for k in range(others):
+        serve(0, 0, k)
+    for k in range(others):
+        serve(0, 1, k)
+    t_near.wait_recv()
+    t_pass.start()
+    y_arrival(1).wait_recv()
+    start_z(1, 1)
+    start_z(2, 0)
+    t_pass.wait_recv()
+    normalize(tok_got, seq)
+    all_x_arrivals(0)
+    own_copy(0).wait()
+
+    columns = branches.shape[1]
+    col_tiles = columns // PIECE
+
+    def branch_step(index, carry):
+        row = aligned((index // col_tiles) * seq, 64)
+        col = aligned(lax.rem(index, col_tiles) * PIECE, PIECE)
+        value = jnp.dot(normed[pl.ds(row, seq), :], b_full[:, pl.ds(col, PIECE)], preferred_element_type=F32)
+        branches[pl.ds(row, seq), pl.ds(col, PIECE)] = (value * scales[:, pl.ds(col, PIECE)]).astype(BF16)
+        serve_step(1, index)
+        return carry
+
+    lax.fori_loop(0, 2 * col_tiles, branch_step, 0)
+
+    groups = columns // 2 // LANES
+
+    def mixer_step(index, carry):
+        row = aligned((index // groups) * seq, 64)
+        group = lax.rem(index, groups)
+        col = aligned(group * LANES, LANES)
+        lanes = pl.ds(col, LANES)
+        mixed[pl.ds(row, seq), lanes] = mixer_group(
+            branches[pl.ds(row, seq), lanes].astype(F32),
+            branches[pl.ds(row, seq), pl.ds(aligned(columns // 2 + col, LANES), LANES)].astype(F32),
+            taps[:, lanes], recur_map[lanes, :], input_map[lanes, :], rate[:, lanes],
+        )
+
+        @pl.when(index == groups)
+        def _():
+            y_arrival(2).wait_recv()
+            start_z(2, 1)
+            start_z(3, 0)
+
+        @pl.when(index > groups)
+        def _():
+            serve_step(2, index - groups - 1, others)
+
+        return carry
+
+    lax.fori_loop(0, 2 * groups, mixer_step, 0)
+    y_arrival(3).wait_recv()
+    start_z(3, 1)
+
+    def block_of(index):
+        item = index - 2
+        kind = (item + 2 * others) // others - 2
+        far = item_slot(lax.rem(kind + 2, 2), lax.rem(item + 2 * others, others))
+        near = z * 2 + lax.rem(y + index, 2)
+        late = (index + shards - 2) // shards
+        return near + late * (far - near)
+
+    def near_copy(phase, block):
+        return push(give.at[block], got_near.at[block], n_sent.at[phase, block], n_land.at[phase, block], core_peer)
+
+    def far_copy(phase, block):
+        return push(stage.at[block], got_far.at[block], f_sent.at[phase, block], f_land.at[phase, block], y_peer)
+
+    def project(phase, w, lhs, before):
+        depth_rows = parts[w].shape[1]
+
+        def combine(index):
+            block = block_of(index)
+            near_copy(phase, block).wait_recv()
+            stage[block] = (keep[block] + got_near[block, 1].astype(F32)).astype(BF16)
+            total[block] += got_near[block, 0].astype(F32)
+            far_copy(phase, block).start()
+
+        def body(index, carry):
+            before(index)
+            block = block_of(index)
+            weight = fulls[w][pl.ds(aligned(block * depth_rows, 64), depth_rows), :]
+            for side in range(2):
+                left = lhs[pl.ds(aligned(side * seq + (1 - core) * share, 64), share), :]
+                give[block, side] = jnp.dot(left, weight, preferred_element_type=F32).astype(BF16)
+            own = lhs[pl.ds(aligned(core * share, 64), share), :]
+            total[block] = jnp.dot(own, weight, preferred_element_type=F32)
+            near_copy(phase, block).start()
+            own = lhs[pl.ds(aligned(seq + core * share, 64), share), :]
+            keep[block] = jnp.dot(own, weight, preferred_element_type=F32)
+
+            @pl.when(index > 0)
+            def _():
+                combine(index - 1)
+
+            return carry
+
+        lax.fori_loop(0, shards, body, 0)
+        combine(shards - 1)
+
+    def collect(phase, between):
+        def body(index, carry):
+            block = block_of(index)
+            far_copy(phase, block).wait_recv()
+            total[block] += got_far[block].astype(F32)
+            between(index)
+            return carry
+
+        lax.fori_loop(0, shards, body, 0)
+
+        def drain(index, carry):
+            far_copy(phase, index).wait_send()
+            near_copy(phase, index).wait_send()
+            return carry
+
+        lax.fori_loop(0, shards, drain, 0)
+
+    all_x_arrivals(1)
+    own_copy(1).wait()
+    project(0, 1, mixed, lambda index: None)
+
+    def serve_up(index):
+        @pl.when(lax.rem(index, 2) == 1)
+        def _():
+            serve_step(2, others + index // 2)
+
+    collect(0, serve_up)
+
+    own_gains.wait()
+    for step in range(1, shards):
+        source = lax.rem(me + step, shards)
+        push(gains, gains_full.at[source], g_sent.at[step - 1], g_land.at[source], y_peer).wait_recv()
+
+    def summed(start):
+        values = [total[block, pl.ds(start, rows), :] for block in range(shards)]
+        squares = sum(jnp.sum(value * value, axis=-1, keepdims=True) for value in values)
+        return values, lax.rsqrt(squares * (1.0 / width) + EPSILON)
+
+    pieces = m_sent.shape[0]
+    piece_rows = share // pieces
+
+    def piece(ref, base, index):
+        return ref.at[pl.ds(aligned(base + index * piece_rows, 16), piece_rows)]
+
+    def to_far(index):
+        return push(
+            piece(mlp_in, core * share, index), piece(mlp_in, seq + core * share, index),
+            m_sent.at[index], m_land.at[index], y_peer,
+        )
+
+    def to_near(index):
+        block = piece(mlp_in, core * share, index)
+        return push(block, block, mn_sent.at[index], mn_land.at[index], core_peer)
+
+    def onward(index):
+        block = piece(mlp_in, seq + core * share, index)
+        return push(block, block, mf_sent.at[index], mf_land.at[index], core_peer)
+
+    def entry_piece(index, carry):
+        def entry_rows(inner, inner_carry):
+            start = aligned(index * piece_rows + inner * rows, rows)
+            values, factor = summed(start)
+            place = aligned(core * share + start, rows)
+            squares = jnp.zeros((rows, 1), F32)
+            kept = []
+            for block in range(shards):
+                cols = pl.ds(block * PIECE, PIECE)
+                value = tokens[pl.ds(place, rows), cols].astype(F32) + values[block] * factor * gains_full[block, 0:1, :]
+                value = value.astype(BF16)
+                hidden[pl.ds(start, rows), cols] = value
+                value = value.astype(F32)
+                kept.append(value)
+                squares += jnp.sum(value * value, axis=-1, keepdims=True)
+            scale = lax.rsqrt(squares * (1.0 / width) + EPSILON)
+            for block in range(shards):
+                mlp_in[pl.ds(place, rows), pl.ds(block * PIECE, PIECE)] = (kept[block] * scale).astype(BF16)
+            return inner_carry
+
+        lax.fori_loop(0, piece_rows // rows, entry_rows, 0)
+        to_far(index).start()
+        to_near(index).start()
+        return carry
+
+    lax.fori_loop(0, pieces, entry_piece, 0)
+    all_x_arrivals(2)
+    own_copy(2).wait()
+
+    def wait_near(index, carry):
+        to_near(index).wait_recv()
+        return carry
+
+    lax.fori_loop(0, pieces, wait_near, 0)
+    up_tiles = active.shape[1] // PIECE
+
+    def up_rows(base):
+        def body(index, carry):
+            col = aligned(index * PIECE, PIECE)
+            value = jnp.dot(mlp_in[pl.ds(base, seq), :], u_full[:, pl.ds(col, PIECE)], preferred_element_type=F32)
+            value = jnp.maximum(value * up_scale[:, pl.ds(col, PIECE)], 0.0)
+            active[pl.ds(base, seq), pl.ds(col, PIECE)] = (value * value).astype(BF16)
+            return carry
+
+        lax.fori_loop(0, up_tiles, body, 0)
+
+    up_rows(0)
+
+    def pass_on(index, carry):
+        to_far(index).wait_recv()
+        onward(index).start()
+        return carry
+
+    lax.fori_loop(0, pieces, pass_on, 0)
+
+    def wait_far(index, carry):
+        onward(index).wait_recv()
+        return carry
+
+    lax.fori_loop(0, pieces, wait_far, 0)
+    up_rows(seq)
+
+    def before_down(index):
+        serve_step(3, index)
+
+        @pl.when(index >= 2)
+        def _():
+            item = index - 2
+            x_arrival(3, item // others, lax.rem(item, others))
+
+    own_copy(3).wait()
+    project(1, 3, active, before_down)
+    collect(1, lambda index: None)
+
+    def last_rows(index, carry):
+        start = aligned(index * rows, rows)
+        values, factor = summed(start)
+        for block in range(shards):
+            cols = pl.ds(block * PIECE, PIECE)
+            value = hidden[pl.ds(start, rows), cols].astype(F32) + values[block] * factor * gains_full[block, 1:2, :]
+            out[pl.ds(start, rows), cols] = value.astype(BF16)
+        return carry
+
+    lax.fori_loop(0, share // rows, last_rows, 0)
+
+    for w in range(WEIGHTS):
+        y_copy(w).wait_send()
+        for kind in range(2):
+            for k in range(others - 1):
+                z_copy(w, kind, k).wait_send()
+
+            @pl.when(depth > 0)
+            def _():
+                z_copy(w, kind, others - 1).wait_send()
+
+            @pl.when(depth == 1)
+            def _():
+                zf_copy(w, kind).wait_send()
+
+            for k in range(others):
+                x_copy(w, kind, k).wait_send()
+    t_near.wait_send()
+    t_pass.wait_send()
+    for step in range(1, shards):
+        gain_copy(step).wait_send()
+
+    def drain(index, carry):
+        to_far(index).wait_send()
+        to_near(index).wait_send()
+        onward(index).wait_send()
+        return carry
+
+    lax.fori_loop(0, pieces, drain, 0)
+
+
+def layer(shards, tokens, gains, weight_parts, scales, up_scale, taps, recur_map, input_map, rate):
+    seq, width = tokens.shape
+    share = seq // 2
+    lines = shards // 2
+    pieces = 4
+    branch_width, hidden_units = scales.shape[1], up_scale.shape[1]
+    dma = pltpu.SemaphoreType.DMA
+    vmem = pl.BlockSpec(memory_space=pltpu.VMEM)
+    anywhere = pl.BlockSpec(memory_space=pl.ANY)
+    fulls = [pltpu.VMEM((shards * part.shape[1], part.shape[2]), BF16) for part in weight_parts]
+    return pl.pallas_call(
+        functools.partial(layer_kernel, shards),
+        out_shape=jax.ShapeDtypeStruct((share, width), BF16),
+        in_specs=[vmem, vmem] + [anywhere] * WEIGHTS + [vmem] * 6,
+        out_specs=vmem,
+        scratch_shapes=fulls + [
+            pltpu.VMEM((shards,) + gains.shape, F32),
+            pltpu.VMEM((seq, width), BF16),
+            pltpu.VMEM((2 * seq, width), BF16),
+            pltpu.VMEM((2 * seq, branch_width), BF16),
+            pltpu.VMEM((2 * seq, branch_width // 2), BF16),
+            pltpu.VMEM((2 * seq, width), BF16),
+            pltpu.VMEM((2 * seq, hidden_units), BF16),
+            pltpu.VMEM((share, width), BF16),
+            pltpu.VMEM((shards, 2, share, width // shards), BF16),
+            pltpu.VMEM((shards, 2, share, width // shards), BF16),
+            pltpu.VMEM((shards, share, width // shards), F32),
+            pltpu.VMEM((shards, share, width // shards), F32),
+            pltpu.VMEM((shards, share, width // shards), BF16),
+            pltpu.VMEM((shards, share, width // shards), BF16),
+            dma((WEIGHTS,)), dma((WEIGHTS,)), dma((WEIGHTS,)),
+            dma((WEIGHTS, 2, lines - 1)), dma((WEIGHTS, shards)), dma((WEIGHTS, 2)),
+            dma((WEIGHTS, 2, lines - 1)), dma((WEIGHTS, shards)),
+            dma, dma((shards - 1,)), dma((shards,)),
+            dma((2,)), dma((2,)),
+            dma((2, shards)), dma((2, shards)), dma((2, shards)), dma((2, shards)),
+            dma((pieces,)), dma((pieces,)), dma((pieces,)), dma((pieces,)), dma((pieces,)), dma((pieces,)),
+        ],
+        compiler_params=pltpu.CompilerParams(
+            collective_id=4, has_side_effects=True, vmem_limit_bytes=66_000_000
+        ),
+        cost_estimate=pl.CostEstimate(flops=20_000_000_000, bytes_accessed=80_000_000, transcendentals=0),
+        name="layer",
+    )(tokens, gains, *weight_parts, scales, up_scale, taps, recur_map, input_map, rate)
+
+
+def on_device_paired(
+    tokens, gain_mix_pre, gain_mix_post, gain_mlp_pre, gain_mlp_post,
+    x_weight, gate_weight, x_scale, gate_scale, conv_weight, recur_map, input_map,
+    decay_param, out_weight, out_scale, up_weight, up_scale, down_weight, down_scale,
+):
+    shards = lax.axis_size("fs")
+    side = lax.rem(lax.axis_index("fs"), 2)
+
+    def part(values, axis):
+        size = values.shape[axis] // 2
+        return lax.dynamic_slice_in_dim(values, side * size, size, axis)
+
+    def by_columns(*arrays):
+        halves = [jnp.split(array, 2, axis=1) for array in arrays]
+        return jnp.stack([jnp.concatenate([pair[p] for pair in halves], axis=1) for p in range(2)])
+
+    def by_rows(array):
+        return array.reshape(2, array.shape[0] // 2, array.shape[1])
+
+    pre, mlp_pre = gain_mix_pre[:, None], gain_mlp_pre[:, None]
+    weight_parts = (
+        by_columns((x_weight * pre).astype(BF16), (gate_weight * pre).astype(BF16)),
+        by_rows((out_weight * out_scale).astype(BF16)),
+        by_columns((up_weight * mlp_pre).astype(BF16)),
+        by_rows((down_weight * down_scale).astype(BF16)),
+    )
+    gains = jnp.stack([gain_mix_post, gain_mlp_post])
+    scales = jnp.concatenate([part(x_scale, 0), part(gate_scale, 0)])[None]
+    width = scales.shape[1] // 2
+
+    def dense(block_map):
+        rows = lax.broadcasted_iota(jnp.int32, (width, LANES), 0)
+        columns = lax.broadcasted_iota(jnp.int32, (width, LANES), 1)
+        spread = jnp.tile(part(block_map, 0), (1, LANES // BLOCK))
+        return jnp.where(rows % LANES // BLOCK == columns // BLOCK, spread, 0).astype(BF16)
+
+    rate = (-DECAY_SCALE * jax.nn.softplus(-part(decay_param, 0)))[None]
+    return layer(
+        shards, tokens[0], gains, weight_parts, scales, part(up_scale, 0)[None], part(conv_weight, 1),
+        dense(recur_map), dense(input_map), rate,
+    )[None]
+
+
 def solution(mesh):
     in_specs = (
         P(("rep", "fs"), None, None),
@@ -353,6 +888,10 @@
         P("tp", "fs"), P("fs"),
     )
     out_specs = P(("rep", "fs"), "tp", None)
+    paired = (
+        mesh.shape["rep"] == 2 and mesh.shape["tp"] == 2
+        and mesh.shape["fs"] % 4 == 0 and mesh.shape["fs"] > 4
+    )
     return jax.shard_map(
-        on_device, mesh=mesh, in_specs=in_specs, out_specs=out_specs, check_vma=False
+        on_device_paired if paired else on_device, mesh=mesh, in_specs=in_specs, out_specs=out_specs, check_vma=False
     )

time: 380 us -> 260 us (0.68)
  waiting for transfers between devices: 63.5 us -> 0 us
  matrix products: 35.4 us -> 0 us
  between operations: 13.4 us -> 0.17 us
  other arithmetic: 20.8 us -> 10.5 us
  local copies, waits for them, and re-layouts: 1.83 us -> 9.23 us
  Pallas kernels: 244 us -> 239 us
    all_gather x3 -> x0, waiting for transfers between devices: 62.8 us -> none  [the longest x1 41.6 us: on_device(): branch_full = lax.all_gather(branch_rows, 'fs', axis=0, tiled=True)]
    dot_general x3 -> x0, matrix products: 35.4 us -> none  [the longest x1 19.9 us: on_device(): jnp.dot(activated, down_full, preferred_element_type=F32).astype(BF16)]
    convert_element_type x8 -> x4, other arithmetic: 10.3 us -> 3.58 us  [the longest x1 1.56 us: on_device_paired(): (out_weight * out_scale).astype(BF16)]
    reduce_sum x4 -> x0, other arithmetic: 4.9 us -> none  [unit_rows(): jnp.mean(values * values, axis=-1, keepdims=True) + EPSILON]
    pallas_call x6 -> x1, Pallas kernels: 244 us -> 239 us  [layer(): pl.pallas_call(functools.partial(layer_kernel, shards), out_shape=jax.Sha...]
    another operation x0 -> x5, other arithmetic: none -> 3.93 us  [the longest x4 2.49 us: by_columns(): jnp.stack([jnp.concatenate([pair[p] for pair in halves], axis=1) for p in...]
    unnamed x28 -> x19, local copies, waits for them, and re-layouts: 0.63 us -> 4.52 us
  transfers between devices with their start and end apart: 3 -> 0, of which waited for: 2 -> 0; matrix products, arithmetic and copies ran while one was open for 8% -> 0% of each run, Pallas kernels for 55% -> 0%
where the time goes in v1:
time: 260 us; the launch traced here: 259 us
  Pallas kernels  239 us (92%)
  other arithmetic  10.5 us (4%)
  local copies, waits for them, and re-layouts  9.23 us (4%)
    pallas_call x1, Pallas kernels, layer(): pl.pallas_call(functools.partial(layer_kernel, shards), out_shape=jax.Sha...  239 us

profile of v1, /device:TPU:0, one launch (start us, length us, event | category | flops | bytes accessed | tf_op | source)
XLA Modules:
  0.0 259.4 jit_solution(16605823085926255235)
XLA Ops:
  0.1 1.4 pad_maximum_fusion.3.gains
  1.5 0.8 dynamic_slice.21
  2.3 0.8 dynamic_slice.22
  3.0 0.6 pad_maximum_fusion.2
  3.6 1.3 fusion.6
  5.0 0.8 dynamic_slice.23
  5.7 0.6 broadcast_in_dim.22.up_scale
  6.3 0.6 constant_dynamic-slice_fusion.2.taps
  6.9 0.8 constant_dynamic-slice_fusion
  7.7 0.1 copy.23
  7.9 0.1 copy.22
  8.0 1.0 broadcast_select_fusion
  9.0 1.6 multiply_convert_fusion.2
  10.6 0.2 multiply_convert_fusion.4
  10.8 0.1 fusion.11
  11.1 1.1 pad_maximum_fusion.1.b_parts
  12.1 1.0 copy-done.1
  13.2 0.4 multiply_convert_fusion.1
  13.6 0.1 slice_bitcast_fusion.1
  13.7 1.3 pad_maximum_fusion.u_parts
  15.0 1.1 copy-done.2
  16.1 1.4 multiply_convert_fusion
  17.6 239.5 %layer.1 = bf16[256,2048]{1,0:T(8,128)(2,1)} custom-call(bf16[512,2048]{1,0:T(8,128)(2,1)} %bitcast.27, f32[2,256]{1,0:T(2,128)} %pad_maximum_fusion.3.gains, bf16[2,256,1024]{2,1,0:T(8,128)(2,1)} %pad_maximum_fusion.1.b_parts, bf16[2,512,256]{2,1,0:T(8,128)(2,1)} %bitcast.22, bf16[2,256,1536]{2,1,0:T(8,128)(2,1)} %pad_maximum_fusion.u_parts, ...), custom_call_target="tpu_custom_call" | custom-call | flops 20000000000 | bytes 80000000 | tf_op jit(solution)/shard_map/layer/pallas_call | solution.py:800
  257.1 2.3 copy.25
  (24 shorter events, 0.2 us)
Async XLA Ops:
  0.0 6.3 %copy-start = (f32[4,1024]{1,0:T(4,128)S(1)}, f32[4,1024]{1,0:T(4,128)}, u32[]{:S(2)}) copy-start(f32[4,1024]{1,0:T(4,128)} %param.28) | copy-start | bytes 49156
  0.0 9.0 %copy-start.3 = (f32[1024,256]{1,0:T(8,128)S(1)}, f32[1024,256]{1,0:T(8,128)}, u32[]{:S(2)}) copy-start(f32[1024,256]{1,0:T(8,128)} %param.32) | copy-start | bytes 3145732
  0.0 10.6 %copy-start.4 = (f32[256,1024]{1,0:T(8,128)S(1)}, f32[256,1024]{1,0:T(8,128)}, u32[]{:S(2)}) copy-start(f32[256,1024]{1,0:T(8,128)} %param.24) | copy-start | bytes 3145732
  0.0 10.6 %copy-start.6 = (f32[256]{0:T(256)S(1)}, f32[256]{0:T(256)}, u32[]{:S(2)}) copy-start(f32[256]{0:T(256)} %param.20) | copy-start | bytes 3076
  8.0 2.6 %copy-start.5 = (f32[256,1024]{1,0:T(8,128)S(1)}, f32[256,1024]{1,0:T(8,128)}, u32[]{:S(2)}) copy-start(f32[256,1024]{1,0:T(8,128)} %param.25) | copy-start | bytes 3145732
  10.9 2.3 copy-start.1
  10.9 2.3 copy-start.7
  13.7 2.5 copy-start.2
  13.7 2.5 copy-start.8

commit v2 on v1

--- a/solution.py
+++ b/solution.py
@@ -345,20 +345,24 @@
 PIECE = 256
 
 
-def mixer_group(x_branch, gate, taps, recur_map, input_map, rate):
+def log_decay_and_drive(conv, logits, rate):
+    lanes = conv.shape[1]
+    log_decay = jax.nn.sigmoid(logits[:, :lanes]) * rate
+    decay = jnp.exp(log_decay)
+    z = -2.0 * log_decay
+    series = z * (1.0 - z * (1 / 2) * (1.0 - z * (1 / 3) * (1.0 - z * (1 / 4) * (1.0 - z * (1 / 5)))))
+    power = jnp.where(z < 0.1, series, 1.0 - decay * decay)
+    return decay, jnp.sqrt(power) * jax.nn.sigmoid(logits[:, lanes:]) * conv.astype(F32)
+
+
+def mixer_group(x_branch, gate, taps, maps, rate):
     length, count = x_branch.shape[0], taps.shape[0]
     total = taps[count - 1 : count, :] * x_branch
     for tap in range(count - 1):
         total += taps[tap : tap + 1, :] * shifted(x_branch, count - 1 - tap, 0.0)
     conv = total.astype(BF16)
-    recur = jax.nn.sigmoid(jnp.dot(conv, recur_map, preferred_element_type=F32))
-    gate_in = jax.nn.sigmoid(jnp.dot(conv, input_map, preferred_element_type=F32))
-    log_decay = recur * rate
-    decay = jnp.exp(log_decay)
-    z = -2.0 * log_decay
-    series = z * (1.0 - z * (1 / 2) * (1.0 - z * (1 / 3) * (1.0 - z * (1 / 4) * (1.0 - z * (1 / 5)))))
-    power = jnp.where(z < 0.1, series, 1.0 - decay * decay)
-    state = jnp.sqrt(power) * gate_in * conv.astype(F32)
+    logits = lax.dot_general(conv, maps, (((1,), (1,)), ((), ())), preferred_element_type=F32)
+    decay, state = log_decay_and_drive(conv, logits, rate)
     distance = 1
     while distance < length:
         state = state + decay * shifted(state, distance, 0.0)
@@ -367,15 +371,27 @@
     return (state * jax.nn.gelu(gate)).astype(BF16)
 
 
+def softplus_of_negative(values):
+    small = jnp.exp(-jnp.abs(values))
+    series = jnp.zeros_like(small)
+    for term in range(8, 0, -1):
+        series = small * (1.0 / term - series)
+    return jnp.maximum(-values, 0.0) + jnp.where(small < 0.1, series, jnp.log(1.0 + small))
+
+
 def aligned(start, unit):
     return pl.multiple_of(start, unit)
 
 
 def layer_kernel(
-    shards, tokens, gains, b_parts, o_parts, u_parts, d_parts, scales, up_scale, taps, recur_map, input_map, rate,
-    out, b_full, o_full, u_full, d_full, gains_full, tok_got, normed, branches, mixed, mlp_in, active, hidden,
+    shards, tokens, mix_pre, mix_post, mlp_pre, mlp_post, out_scale, down_scale,
+    x_scale, gate_scale, up_scale, conv_weight, recur_map, input_map, decay_param,
+    x_weight, gate_weight, out_weight, up_weight, down_weight, out,
+    b_full, o_full, u_full, d_full, b_give, o_give, u_give, d_give,
+    x_raw, gate_raw, o_raw, u_raw, d_raw, gains_full, gain_rows, scales, maps, rate,
+    tok_got, normed, branches, mixed, mlp_in, active, hidden,
     give, got_near, keep, total, stage, got_far,
-    own_sem, y_sent, y_land, z_sent, z_land, zf_sent, x_sent, x_land, g_own, g_sent, g_land,
+    raw_sem, y_sent, y_land, z_sent, z_land, zf_sent, x_sent, x_land, g_sent, g_land,
     t_sent, t_land, n_sent, n_land, f_sent, f_land, m_sent, m_land, mn_sent, mn_land, mf_sent, mf_land,
 ):
     lines = shards // 2
@@ -385,117 +401,192 @@
     x_peer, core_peer, y_peer = {"rep": 1 - rep}, {"tp": 1 - core}, {"fs": z * 2 + 1 - y}
     upper = z // (lines // 2)
     depth = z + upper * (lines - 1 - 2 * z)
+    inner = (depth + lines - 1) // lines
 
     def other(k):
-        place = k + (k + lines - depth) // lines
+        turned = lax.rem(k + inner * (others - 1), others)
+        place = turned + (turned + lines - depth) // lines
         return place + upper * (lines - 1 - 2 * place)
 
-    greet(
-        [{"fs": lax.rem(me + step, shards)} for step in range(1, shards)] + [x_peer, core_peer]
-    )
-    parts = (b_parts, o_parts, u_parts, d_parts)
+    seq, width = tokens.shape
+    share = seq // 2
+    columns = branches.shape[1]
+    channels = columns // 2
+    units = active.shape[1]
+    gives = (b_give, o_give, u_give, d_give)
     fulls = (b_full, o_full, u_full, d_full)
 
+    raw_copies = [
+        pltpu.make_async_copy(x_weight, x_raw, raw_sem.at[0]),
+        pltpu.make_async_copy(gate_weight, gate_raw, raw_sem.at[1]),
+        pltpu.make_async_copy(out_weight, o_raw, raw_sem.at[2]),
+        pltpu.make_async_copy(up_weight, u_raw, raw_sem.at[3]),
+        pltpu.make_async_copy(down_weight, d_raw, raw_sem.at[4]),
+    ]
+    for copy in raw_copies:
+        copy.start()
+    peers = [{"fs": lax.rem(me + step, shards)} for step in range(1, shards)] + [x_peer, core_peer]
+    barrier = pltpu.get_barrier_semaphore()
+    for peer in peers:
+        pl.semaphore_signal(barrier, inc=1, device_id=peer, device_id_type=MESH_IDS)
+    for row, gain in enumerate((mix_pre, mix_post, mlp_pre, mlp_post)):
+        gains_full[me, row : row + 1, :] = gain[...]
+    chunk = 32
+
+    def cast(count, move):
+        def body(index, carry):
+            move(aligned(index * chunk, chunk))
+            return carry
+
+        lax.fori_loop(0, count // chunk, body, 0)
+
+    def branch_rows(start):
+        rows = pl.ds(start, chunk)
+        home = pl.ds(aligned(me * b_give.shape[0] + start, chunk), chunk)
+        for at, raw in enumerate((x_raw, gate_raw)):
+            place = pl.ds(at * channels, channels)
+            b_full[home, place] = raw[rows, pl.ds(aligned(y * channels, LANES), channels)].astype(BF16)
+            b_give[rows, place] = raw[rows, pl.ds(aligned((1 - y) * channels, LANES), channels)].astype(BF16)
+
+    def up_rows_cast(start):
+        rows = pl.ds(start, chunk)
+        home = pl.ds(aligned(me * u_give.shape[0] + start, chunk), chunk)
+        u_full[home, :] = u_raw[rows, pl.ds(aligned(y * units, LANES), units)].astype(BF16)
+        u_give[rows, :] = u_raw[rows, pl.ds(aligned((1 - y) * units, LANES), units)].astype(BF16)
+
+    def column_rows(full, spare, raw, scale):
+        size = spare.shape[0]
+
+        def move(start):
+            home = pl.ds(aligned(me * size + start, chunk), chunk)
+            full[home, :] = (raw[pl.ds(aligned(y * size + start, chunk), chunk), :] * scale[...]).astype(BF16)
+            rows = pl.ds(start, chunk)
+            spare[rows, :] = (raw[pl.ds(aligned((1 - y) * size + start, chunk), chunk), :] * scale[...]).astype(BF16)
+
+        return move
+
     def half(w, slot, side):
-        rows = parts[w].shape[1]
+        rows = gives[w].shape[0]
         return fulls[w].at[pl.ds(aligned(slot * rows + side * (rows // 2), 64), rows // 2)]
 
     def whole(w, slot):
-        rows = parts[w].shape[1]
+        rows = gives[w].shape[0]
         return fulls[w].at[pl.ds(aligned(slot * rows, 64), rows)]
 
     def y_copy(w):
-        return push(parts[w].at[1 - y], whole(w, me), y_sent.at[w], y_land.at[w], y_peer)
+        return push(gives[w], whole(w, me), y_sent.at[w], y_land.at[w], y_peer)
 
     def y_arrival(w):
         block = whole(w, z * 2 + 1 - y)
         return push(block, block, y_sent.at[w], y_land.at[w], y_peer)
 
-    def own_copy(w):
-        return pltpu.make_async_copy(parts[w].at[y], whole(w, me), own_sem.at[w])
-
     def z_copy(w, kind, k):
         slot = z * 2 + lax.rem(y + kind, 2)
-        target = half(w, slot, rep)
-        rows = parts[w].shape[1] // 2
-        source = parts[w].at[y, pl.ds(aligned(rep * rows, 64), rows)] if kind == 0 else target
-        return push(source, target, z_sent.at[w, kind, k], z_land.at[w, slot], {"fs": other(k) * 2 + y})
+        block = half(w, slot, rep)
+        return push(block, block, z_sent.at[w, kind, k], z_land.at[w, slot], {"fs": other(k) * 2 + y})
 
     def start_z(w, kind):
-        for k in range(others - 1):
-            z_copy(w, kind, k).start()
-
-        @pl.when(depth > 0)
-        def _():
-            z_copy(w, kind, others - 1).start()
+        z_copy(w, kind, 1).start()
+        z_copy(w, kind, 0).start()
+        for k in range(2, others):
+
+            @pl.when((inner == 1) | (k < others - 1))
+            def _():
+                z_copy(w, kind, k).start()
 
     def item_slot(kind, k):
         return other(k) * 2 + lax.rem(y + kind, 2)
 
     def zf_copy(w, kind):
-        block = half(w, item_slot(kind, others - 1), rep)
-        ends = upper * (lines - 1)
-        return push(block, block, zf_sent.at[w, kind], z_land.at[w, item_slot(kind, others - 1)], {"fs": ends * 2 + y})
+        slot = item_slot(kind, 0)
+        block = half(w, slot, rep)
+        return push(block, block, zf_sent.at[w, kind], z_land.at[w, slot], {"fs": upper * (lines - 1) * 2 + y})
 
     def x_copy(w, kind, k):
         slot = item_slot(kind, k)
         block = half(w, slot, rep)
         return push(block, block, x_sent.at[w, kind, k], x_land.at[w, slot], x_peer)
 
-    def serve(w, kind, k):
+    def serve(w, item):
+        kind, k = item // others, lax.rem(item, others)
         slot = item_slot(kind, k)
         block = half(w, slot, rep)
         push(block, block, x_sent.at[w, kind, k], z_land.at[w, slot], x_peer).wait_recv()
+
+        @pl.when((k == 0) & (depth == 1))
+        def _():
+            zf_copy(w, kind).start()
+
         x_copy(w, kind, k).start()
 
-        def onward():
-            zf_copy(w, kind).start()
-
-        if isinstance(k, int):
-            if k == others - 1:
-                pl.when(depth == 1)(onward)
-        else:
-            pl.when((k == others - 1) & (depth == 1))(onward)
-
-    def x_arrival(w, kind, k):
-        slot = item_slot(kind, k)
+    def x_arrival(w, item):
+        slot = item_slot(item // others, lax.rem(item, others))
         block = half(w, slot, 1 - rep)
-        push(block, block, x_sent.at[w, kind, k], x_land.at[w, slot], x_peer).wait_recv()
+        push(block, block, x_sent.at[w, 0, 0], x_land.at[w, slot], x_peer).wait_recv()
+
+    items = 2 * others
 
     def all_x_arrivals(w):
         def body(index, carry):
-            x_arrival(w, index // others, lax.rem(index, others))
+            x_arrival(w, index)
             return carry
 
-        lax.fori_loop(0, 2 * others, body, 0)
-
-    def serve_step(w, index, count=2 * others):
-        @pl.when((index >= 0) & (index < count))
-        def _():
-            serve(w, index // others, lax.rem(index, others))
-
-    seq = tokens.shape[0]
-    share = seq // 2
-    width = tokens.shape[1]
+        lax.fori_loop(0, items, body, 0)
+
+    def when(condition, act):
+        pl.when(condition)(act)
+
     mine = pl.ds(aligned(core * share, 64), share)
     t_near = push(tokens.at[mine], tok_got.at[mine], t_sent.at[0], t_land.at[0], y_peer)
     t_pass = push(tok_got.at[mine], tok_got.at[mine], t_sent.at[1], t_land.at[1], core_peer)
 
+    def gain_copy(step):
+        block = gains_full.at[me]
+        return push(block, block, g_sent.at[step - 1], g_land.at[me], {"fs": lax.rem(me + step, shards)})
+
+    raw_copies[0].wait()
+    raw_copies[1].wait()
+    cast(b_give.shape[0], branch_rows)
+    pl.semaphore_wait(barrier, len(peers))
     y_copy(0).start()
     start_z(0, 0)
-    t_near.start()
-    for w in range(1, WEIGHTS):
-        y_copy(w).start()
-    for w in range(WEIGHTS):
-        own_copy(w).start()
-    own_gains = pltpu.make_async_copy(gains, gains_full.at[me], g_own)
-    own_gains.start()
-
-    def gain_copy(step):
-        return push(gains, gains_full.at[me], g_sent.at[step - 1], g_land.at[me], {"fs": lax.rem(me + step, shards)})
-
     for step in range(1, shards):
         gain_copy(step).start()
+    raw_copies[2].wait()
+    cast(o_give.shape[0], column_rows(o_full, o_give, o_raw, out_scale))
+    raw_copies[3].wait()
+    cast(u_give.shape[0], up_rows_cast)
+    raw_copies[4].wait()
+    cast(d_give.shape[0], column_rows(d_full, d_give, d_raw, down_scale))
+    y_copy(1).start()
+    t_near.start()
+    y_copy(2).start()
+    y_copy(3).start()
+
+    part = pl.ds(aligned(y * channels, LANES), channels)
+    scales[:, :channels] = x_scale[:, part]
+    scales[:, channels:] = gate_scale[:, part]
+    rate[...] = -DECAY_SCALE * softplus_of_negative(decay_param[:, part])
+    block_rows = recur_map.shape[0]
+    groups = channels // LANES
+    same = (
+        lax.broadcasted_iota(jnp.int32, (LANES, LANES), 0) // block_rows
+        == lax.broadcasted_iota(jnp.int32, (LANES, LANES), 1) // block_rows
+    )
+    for group in range(groups):
+        lanes = pl.ds(aligned(y * channels + group * LANES, LANES), LANES)
+        for at, block_map in enumerate((recur_map, input_map)):
+            spread = jnp.concatenate([block_map[:, lanes].astype(F32)] * (LANES // block_rows), axis=0)
+            first = (group * 2 + at) * LANES
+            maps[first : first + LANES, :] = jnp.where(same, spread, 0.0).astype(BF16)
+
+    for step in range(1, shards):
+        source = lax.rem(me + step, shards)
+        block = gains_full.at[source]
+        push(block, block, g_sent.at[step - 1], g_land.at[source], y_peer).wait_recv()
+    piece_cols = width // shards
+    for block in range(shards):
+        gain_rows[:, block * piece_cols : (block + 1) * piece_cols] = gains_full[block]
 
     rows = 16
 
@@ -503,30 +594,28 @@
         def body(index, carry):
             start = aligned(index * rows, rows)
             values = source[pl.ds(start, rows), :].astype(F32)
-            normed[pl.ds(aligned(base + start, rows), rows), :] = unit_rows(values).astype(BF16)
+            values = unit_rows(values) * gain_rows[0:1, :]
+            normed[pl.ds(aligned(base + start, rows), rows), :] = values.astype(BF16)
             return carry
 
         lax.fori_loop(0, seq // rows, body, 0)
 
     normalize(tokens, 0)
+    serve(0, 0)
     y_arrival(0).wait_recv()
     start_z(0, 1)
     start_z(1, 0)
-    for k in range(others):
-        serve(0, 0, k)
-    for k in range(others):
-        serve(0, 1, k)
+    serve(0, 1)
+    serve(0, 2)
+    y_arrival(1).wait_recv()
+    start_z(1, 1)
+    serve(0, 3)
+    serve(0, 4)
+    serve(0, 5)
     t_near.wait_recv()
     t_pass.start()
-    y_arrival(1).wait_recv()
-    start_z(1, 1)
-    start_z(2, 0)
-    t_pass.wait_recv()
-    normalize(tok_got, seq)
     all_x_arrivals(0)
-    own_copy(0).wait()
-
-    columns = branches.shape[1]
+
     col_tiles = columns // PIECE
 
     def branch_step(index, carry):
@@ -534,12 +623,18 @@
         col = aligned(lax.rem(index, col_tiles) * PIECE, PIECE)
         value = jnp.dot(normed[pl.ds(row, seq), :], b_full[:, pl.ds(col, PIECE)], preferred_element_type=F32)
         branches[pl.ds(row, seq), pl.ds(col, PIECE)] = (value * scales[:, pl.ds(col, PIECE)]).astype(BF16)
-        serve_step(1, index)
+        when(index >= 2, lambda: serve(1, index - 2))
         return carry
 
-    lax.fori_loop(0, 2 * col_tiles, branch_step, 0)
-
-    groups = columns // 2 // LANES
+    lax.fori_loop(0, col_tiles, branch_step, 0)
+    t_pass.wait_recv()
+    normalize(tok_got, seq)
+    lax.fori_loop(col_tiles, 2 * col_tiles, branch_step, 0)
+    start_z(2, 0)
+
+    def up_sends():
+        y_arrival(2).wait_recv()
+        start_z(2, 1)
 
     def mixer_step(index, carry):
         row = aligned((index // groups) * seq, 64)
@@ -548,30 +643,20 @@
         lanes = pl.ds(col, LANES)
         mixed[pl.ds(row, seq), lanes] = mixer_group(
             branches[pl.ds(row, seq), lanes].astype(F32),
-            branches[pl.ds(row, seq), pl.ds(aligned(columns // 2 + col, LANES), LANES)].astype(F32),
-            taps[:, lanes], recur_map[lanes, :], input_map[lanes, :], rate[:, lanes],
+            branches[pl.ds(row, seq), pl.ds(aligned(channels + col, LANES), LANES)].astype(F32),
+            conv_weight[:, pl.ds(aligned(y * channels + col, LANES), LANES)],
+            maps[pl.ds(aligned(group * 2 * LANES, LANES), 2 * LANES), :], rate[:, lanes],
         )
-
-        @pl.when(index == groups)
-        def _():
-            y_arrival(2).wait_recv()
-            start_z(2, 1)
-            start_z(3, 0)
-
-        @pl.when(index > groups)
-        def _():
-            serve_step(2, index - groups - 1, others)
-
+        when(index == groups, up_sends)
+        when(index == 2 * groups - 2, lambda: serve(2, 0))
         return carry
 
     lax.fori_loop(0, 2 * groups, mixer_step, 0)
-    y_arrival(3).wait_recv()
-    start_z(3, 1)
 
     def block_of(index):
         item = index - 2
-        kind = (item + 2 * others) // others - 2
-        far = item_slot(lax.rem(kind + 2, 2), lax.rem(item + 2 * others, others))
+        safe = lax.rem(item + items, items)
+        far = item_slot(safe // others, lax.rem(safe, others))
         near = z * 2 + lax.rem(y + index, 2)
         late = (index + shards - 2) // shards
         return near + late * (far - near)
@@ -583,7 +668,7 @@
         return push(stage.at[block], got_far.at[block], f_sent.at[phase, block], f_land.at[phase, block], y_peer)
 
     def project(phase, w, lhs, before):
-        depth_rows = parts[w].shape[1]
+        depth_rows = gives[w].shape[0]
 
         def combine(index):
             block = block_of(index)
@@ -604,11 +689,7 @@
             near_copy(phase, block).start()
             own = lhs[pl.ds(aligned(seq + core * share, 64), share), :]
             keep[block] = jnp.dot(own, weight, preferred_element_type=F32)
-
-            @pl.when(index > 0)
-            def _():
-                combine(index - 1)
-
+            when(index > 0, lambda: combine(index - 1))
             return carry
 
         lax.fori_loop(0, shards, body, 0)
@@ -631,21 +712,17 @@
 
         lax.fori_loop(0, shards, drain, 0)
 
+    def during_sum(index):
+        when(index == 1, lambda: serve(2, 2))
+
+        @pl.when(index == 5)
+        def _():
+            serve(2, 3)
+            start_z(3, 0)
+
     all_x_arrivals(1)
-    own_copy(1).wait()
-    project(0, 1, mixed, lambda index: None)
-
-    def serve_up(index):
-        @pl.when(lax.rem(index, 2) == 1)
-        def _():
-            serve_step(2, others + index // 2)
-
-    collect(0, serve_up)
-
-    own_gains.wait()
-    for step in range(1, shards):
-        source = lax.rem(me + step, shards)
-        push(gains, gains_full.at[source], g_sent.at[step - 1], g_land.at[source], y_peer).wait_recv()
+    project(0, 1, mixed, lambda index: when(index == 4, lambda: serve(2, 1)))
+    collect(0, during_sum)
 
     def summed(start):
         values = [total[block, pl.ds(start, rows), :] for block in range(shards)]
@@ -673,15 +750,15 @@
         return push(block, block, mf_sent.at[index], mf_land.at[index], core_peer)
 
     def entry_piece(index, carry):
-        def entry_rows(inner, inner_carry):
-            start = aligned(index * piece_rows + inner * rows, rows)
+        def entry_rows(inner_index, inner_carry):
+            start = aligned(index * piece_rows + inner_index * rows, rows)
             values, factor = summed(start)
             place = aligned(core * share + start, rows)
             squares = jnp.zeros((rows, 1), F32)
             kept = []
             for block in range(shards):
-                cols = pl.ds(block * PIECE, PIECE)
-                value = tokens[pl.ds(place, rows), cols].astype(F32) + values[block] * factor * gains_full[block, 0:1, :]
+                cols = pl.ds(block * piece_cols, piece_cols)
+                value = tokens[pl.ds(place, rows), cols].astype(F32) + values[block] * factor * gain_rows[1:2, cols]
                 value = value.astype(BF16)
                 hidden[pl.ds(start, rows), cols] = value
                 value = value.astype(F32)
@@ -689,7 +766,8 @@
                 squares += jnp.sum(value * value, axis=-1, keepdims=True)
             scale = lax.rsqrt(squares * (1.0 / width) + EPSILON)
             for block in range(shards):
-                mlp_in[pl.ds(place, rows), pl.ds(block * PIECE, PIECE)] = (kept[block] * scale).astype(BF16)
+                cols = pl.ds(block * piece_cols, piece_cols)
+                mlp_in[pl.ds(place, rows), cols] = (kept[block] * scale * gain_rows[2:3, cols]).astype(BF16)
             return inner_carry
 
         lax.fori_loop(0, piece_rows // rows, entry_rows, 0)
@@ -698,27 +776,31 @@
         return carry
 
     lax.fori_loop(0, pieces, entry_piece, 0)
+    serve(2, 4)
+    y_arrival(3).wait_recv()
+    start_z(3, 1)
+    serve(2, 5)
     all_x_arrivals(2)
-    own_copy(2).wait()
 
     def wait_near(index, carry):
         to_near(index).wait_recv()
         return carry
 
     lax.fori_loop(0, pieces, wait_near, 0)
-    up_tiles = active.shape[1] // PIECE
+    up_tiles = units // PIECE
 
     def up_rows(base):
         def body(index, carry):
             col = aligned(index * PIECE, PIECE)
             value = jnp.dot(mlp_in[pl.ds(base, seq), :], u_full[:, pl.ds(col, PIECE)], preferred_element_type=F32)
-            value = jnp.maximum(value * up_scale[:, pl.ds(col, PIECE)], 0.0)
+            value = jnp.maximum(value * up_scale[:, pl.ds(aligned(y * units + col, PIECE), PIECE)], 0.0)
             active[pl.ds(base, seq), pl.ds(col, PIECE)] = (value * value).astype(BF16)
             return carry
 
         lax.fori_loop(0, up_tiles, body, 0)
 
     up_rows(0)
+    serve(3, 0)
 
     def pass_on(index, carry):
         to_far(index).wait_recv()
@@ -726,6 +808,7 @@
         return carry
 
     lax.fori_loop(0, pieces, pass_on, 0)
+    serve(3, 1)
 
     def wait_far(index, carry):
         onward(index).wait_recv()
@@ -735,14 +818,9 @@
     up_rows(seq)
 
     def before_down(index):
-        serve_step(3, index)
-
-        @pl.when(index >= 2)
-        def _():
-            item = index - 2
-            x_arrival(3, item // others, lax.rem(item, others))
-
-    own_copy(3).wait()
+        when((index >= 2) & (index < items), lambda: serve(3, index))
+        when(index >= 2, lambda: x_arrival(3, index - 2))
+
     project(1, 3, active, before_down)
     collect(1, lambda index: None)
 
@@ -750,8 +828,8 @@
         start = aligned(index * rows, rows)
         values, factor = summed(start)
         for block in range(shards):
-            cols = pl.ds(block * PIECE, PIECE)
-            value = hidden[pl.ds(start, rows), cols].astype(F32) + values[block] * factor * gains_full[block, 1:2, :]
+            cols = pl.ds(block * piece_cols, piece_cols)
+            value = hidden[pl.ds(start, rows), cols].astype(F32) + values[block] * factor * gain_rows[3:4, cols]
             out[pl.ds(start, rows), cols] = value.astype(BF16)
         return carry
 
@@ -760,19 +838,17 @@
     for w in range(WEIGHTS):
         y_copy(w).wait_send()
         for kind in range(2):
-            for k in range(others - 1):
-                z_copy(w, kind, k).wait_send()
-
-            @pl.when(depth > 0)
-            def _():
-                z_copy(w, kind, others - 1).wait_send()
+            for k in range(others):
+                x_copy(w, kind, k).wait_send()
+
+                @pl.when((inner == 1) | (k < others - 1))
+                def _():
+                    z_copy(w, kind, k).wait_send()
 
             @pl.when(depth == 1)
             def _():
                 zf_copy(w, kind).wait_send()
 
-            for k in range(others):
-                x_copy(w, kind, k).wait_send()
     t_near.wait_send()
     t_pass.wait_send()
     for step in range(1, shards):
@@ -785,52 +861,6 @@
         return carry
 
     lax.fori_loop(0, pieces, drain, 0)
-
-
-def layer(shards, tokens, gains, weight_parts, scales, up_scale, taps, recur_map, input_map, rate):
-    seq, width = tokens.shape
-    share = seq // 2
-    lines = shards // 2
-    pieces = 4
-    branch_width, hidden_units = scales.shape[1], up_scale.shape[1]
-    dma = pltpu.SemaphoreType.DMA
-    vmem = pl.BlockSpec(memory_space=pltpu.VMEM)
-    anywhere = pl.BlockSpec(memory_space=pl.ANY)
-    fulls = [pltpu.VMEM((shards * part.shape[1], part.shape[2]), BF16) for part in weight_parts]
-    return pl.pallas_call(
-        functools.partial(layer_kernel, shards),
-        out_shape=jax.ShapeDtypeStruct((share, width), BF16),
-        in_specs=[vmem, vmem] + [anywhere] * WEIGHTS + [vmem] * 6,
-        out_specs=vmem,
-        scratch_shapes=fulls + [
-            pltpu.VMEM((shards,) + gains.shape, F32),
-            pltpu.VMEM((seq, width), BF16),
-            pltpu.VMEM((2 * seq, width), BF16),
-            pltpu.VMEM((2 * seq, branch_width), BF16),
-            pltpu.VMEM((2 * seq, branch_width // 2), BF16),
-            pltpu.VMEM((2 * seq, width), BF16),
-            pltpu.VMEM((2 * seq, hidden_units), BF16),
-            pltpu.VMEM((share, width), BF16),
-            pltpu.VMEM((shards, 2, share, width // shards), BF16),
-            pltpu.VMEM((shards, 2, share, width // shards), BF16),
-            pltpu.VMEM((shards, share, width // shards), F32),
-            pltpu.VMEM((shards, share, width // shards), F32),
-            pltpu.VMEM((shards, share, width // shards), BF16),
-            pltpu.VMEM((shards, share, width // shards), BF16),
-            dma((WEIGHTS,)), dma((WEIGHTS,)), dma((WEIGHTS,)),
-            dma((WEIGHTS, 2, lines - 1)), dma((WEIGHTS, shards)), dma((WEIGHTS, 2)),
-            dma((WEIGHTS, 2, lines - 1)), dma((WEIGHTS, shards)),
-            dma, dma((shards - 1,)), dma((shards,)),
-            dma((2,)), dma((2,)),
-            dma((2, shards)), dma((2, shards)), dma((2, shards)), dma((2, shards)),
-            dma((pieces,)), dma((pieces,)), dma((pieces,)), dma((pieces,)), dma((pieces,)), dma((pieces,)),
-        ],
-        compiler_params=pltpu.CompilerParams(
-            collective_id=4, has_side_effects=True, vmem_limit_bytes=66_000_000
-        ),
-        cost_estimate=pl.CostEstimate(flops=20_000_000_000, bytes_accessed=80_000_000, transcendentals=0),
-        name="layer",
-    )(tokens, gains, *weight_parts, scales, up_scale, taps, recur_map, input_map, rate)
 
 
 def on_device_paired(
@@ -839,41 +869,63 @@
     decay_param, out_weight, out_scale, up_weight, up_scale, down_weight, down_scale,
 ):
     shards = lax.axis_size("fs")
-    side = lax.rem(lax.axis_index("fs"), 2)
-
-    def part(values, axis):
-        size = values.shape[axis] // 2
-        return lax.dynamic_slice_in_dim(values, side * size, size, axis)
-
-    def by_columns(*arrays):
-        halves = [jnp.split(array, 2, axis=1) for array in arrays]
-        return jnp.stack([jnp.concatenate([pair[p] for pair in halves], axis=1) for p in range(2)])
-
-    def by_rows(array):
-        return array.reshape(2, array.shape[0] // 2, array.shape[1])
-
-    pre, mlp_pre = gain_mix_pre[:, None], gain_mlp_pre[:, None]
-    weight_parts = (
-        by_columns((x_weight * pre).astype(BF16), (gate_weight * pre).astype(BF16)),
-        by_rows((out_weight * out_scale).astype(BF16)),
-        by_columns((up_weight * mlp_pre).astype(BF16)),
-        by_rows((down_weight * down_scale).astype(BF16)),
-    )
-    gains = jnp.stack([gain_mix_post, gain_mlp_post])
-    scales = jnp.concatenate([part(x_scale, 0), part(gate_scale, 0)])[None]
-    width = scales.shape[1] // 2
-
-    def dense(block_map):
-        rows = lax.broadcasted_iota(jnp.int32, (width, LANES), 0)
-        columns = lax.broadcasted_iota(jnp.int32, (width, LANES), 1)
-        spread = jnp.tile(part(block_map, 0), (1, LANES // BLOCK))
-        return jnp.where(rows % LANES // BLOCK == columns // BLOCK, spread, 0).astype(BF16)
-
-    rate = (-DECAY_SCALE * jax.nn.softplus(-part(decay_param, 0)))[None]
-    return layer(
-        shards, tokens[0], gains, weight_parts, scales, part(up_scale, 0)[None], part(conv_weight, 1),
-        dense(recur_map), dense(input_map), rate,
-    )[None]
+    seq, width = tokens.shape[1:]
+    share, lines, pieces = seq // 2, shards // 2, 4
+    fan_in, channels, units = x_weight.shape[0], x_weight.shape[1] // 2, up_weight.shape[1] // 2
+    piece_cols = width // shards
+    dma = pltpu.SemaphoreType.DMA
+    vmem = pl.BlockSpec(memory_space=pltpu.VMEM)
+    anywhere = pl.BlockSpec(memory_space=pl.ANY)
+    part_shapes = ((fan_in, 2 * channels), (channels, piece_cols), (fan_in, units), (units, piece_cols))
+    raws = (x_weight, gate_weight, out_weight, up_weight, down_weight)
+    rows = [
+        value[None] for value in (
+            gain_mix_pre, gain_mix_post, gain_mlp_pre, gain_mlp_post, out_scale, down_scale,
+            x_scale, gate_scale, up_scale,
+        )
+    ]
+    result = pl.pallas_call(
+        functools.partial(layer_kernel, shards),
+        out_shape=jax.ShapeDtypeStruct((share, width), BF16),
+        in_specs=[vmem] * 14 + [anywhere] * len(raws),
+        out_specs=vmem,
+        scratch_shapes=[pltpu.VMEM((shards * shape[0], shape[1]), BF16) for shape in part_shapes]
+        + [pltpu.VMEM(shape, BF16) for shape in part_shapes]
+        + [pltpu.VMEM(raw.shape, F32) for raw in raws]
+        + [
+            pltpu.VMEM((shards, 4, piece_cols), F32),
+            pltpu.VMEM((4, width), F32),
+            pltpu.VMEM((1, 2 * channels), F32),
+            pltpu.VMEM((2 * channels, LANES), BF16),
+            pltpu.VMEM((1, channels), F32),
+            pltpu.VMEM((seq, width), BF16),
+            pltpu.VMEM((2 * seq, width), BF16),
+            pltpu.VMEM((2 * seq, 2 * channels), BF16),
+            pltpu.VMEM((2 * seq, channels), BF16),
+            pltpu.VMEM((2 * seq, width), BF16),
+            pltpu.VMEM((2 * seq, units), BF16),
+            pltpu.VMEM((share, width), BF16),
+            pltpu.VMEM((shards, 2, share, piece_cols), BF16),
+            pltpu.VMEM((shards, 2, share, piece_cols), BF16),
+            pltpu.VMEM((shards, share, piece_cols), F32),
+            pltpu.VMEM((shards, share, piece_cols), F32),
+            pltpu.VMEM((shards, share, piece_cols), BF16),
+            pltpu.VMEM((shards, share, piece_cols), BF16),
+            dma((len(raws),)), dma((WEIGHTS,)), dma((WEIGHTS,)),
+            dma((WEIGHTS, 2, lines - 1)), dma((WEIGHTS, shards)), dma((WEIGHTS, 2)),
+            dma((WEIGHTS, 2, lines - 1)), dma((WEIGHTS, shards)),
+            dma((shards - 1,)), dma((shards,)),
+            dma((2,)), dma((2,)),
+            dma((2, shards)), dma((2, shards)), dma((2, shards)), dma((2, shards)),
+            dma((pieces,)), dma((pieces,)), dma((pieces,)), dma((pieces,)), dma((pieces,)), dma((pieces,)),
+        ],
+        compiler_params=pltpu.CompilerParams(
+            collective_id=4, has_side_effects=True, vmem_limit_bytes=67_000_000
+        ),
+        cost_estimate=pl.CostEstimate(flops=20_000_000_000, bytes_accessed=80_000_000, transcendentals=0),
+        name="layer",
+    )(tokens[0], *rows, conv_weight, recur_map.T, input_map.T, decay_param[None], *raws)
+    return result[None]
 
 
 def solution(mesh):

time: 260 us -> 228 us (0.88)
  Pallas kernels: 239 us -> 225 us
  other arithmetic: 10.5 us -> 0 us
  local copies, waits for them, and re-layouts: 9.23 us -> 2.3 us
    pallas_call x1, Pallas kernels: 239 us -> 225 us  [on_device_paired(): pl.pallas_call(functools.partial(layer_kernel, shards), out_shape=jax.Sha...]
    another operation x5 -> x0, other arithmetic: 3.93 us -> none  [the longest x4 2.49 us: by_columns(): jnp.stack([jnp.concatenate([pair[p] for pair in halves], axis=1) for p in...]
    dynamic_slice x5 -> x0, local copies, waits for them, and re-layouts: 3.67 us -> none  [part(): return lax.dynamic_slice_in_dim(values, side * size, size, axis)]
    convert_element_type x4 -> x0, other arithmetic: 3.58 us -> none  [the longest x1 1.56 us: on_device_paired(): (out_weight * out_scale).astype(BF16)]
where the time goes in v2:
time: 228 us
  Pallas kernels  225 us (99%)
  local copies, waits for them, and re-layouts  2.3 us (1%)
    pallas_call x1, Pallas kernels, on_device_paired(): pl.pallas_call(functools.partial(layer_kernel, shards), out_shape=jax.Sha...  225 us

profile of v2, /device:TPU:0, one launch (start us, length us, event | category | flops | bytes accessed | tf_op | source)
XLA Modules:
  0.0 227.6 jit_solution(8117524695728215813)
XLA Ops:
  0.0 225.3 %layer.1 = bf16[256,2048]{1,0:T(8,128)(2,1)} custom-call(bf16[512,2048]{1,0:T(8,128)(2,1)} %bitcast.15, f32[1,256]{1,0:T(1,128)} %bitcast.22, f32[1,256]{1,0:T(1,128)} %bitcast.23, f32[1,256]{1,0:T(1,128)} %bitcast.24, f32[1,256]{1,0:T(1,128)} %bitcast.25, f32[1,256]{1,0:T(1,128)} %bitcast.26, f32[1,256]{1,0:T(1,128)} %bitcast.27, f32[1,1024]{1,0:T(1,128)} %bitcast.19, ...), custom_call_target="tpu_custom_call" | custom-call | flops 20000000000 | bytes 80000000 | tf_op jit(solution)/shard_map/layer/pallas_call | solution.py:887
  225.3 2.3 %copy.21 = bf16[1,256,2048]{2,1,0:T(8,128)(2,1)} copy(bf16[1,256,2048]{2,1,0:T(8,128)(2,1)} %bitcast.14) | data formatting | bytes 2097152

commit v3 on v2

--- a/solution.py
+++ b/solution.py
@@ -343,6 +343,7 @@
 
 WEIGHTS = 4
 PIECE = 256
+CUTS = 2
 
 
 def log_decay_and_drive(conv, logits, rate):
@@ -383,16 +384,28 @@
     return pl.multiple_of(start, unit)
 
 
-def layer_kernel(
-    shards, tokens, mix_pre, mix_post, mlp_pre, mlp_post, out_scale, down_scale,
+def layer_kernel(shards, *refs):
+    count = 14
+    sources, raws, out = refs[:count], refs[count : count + 5], refs[count + 5]
+    copies = refs[count + 6 : 2 * count + 6]
+    load_sem = refs[2 * count + 6]
+    loads = [
+        pltpu.make_async_copy(source, copy, load_sem.at[at])
+        for at, (source, copy) in enumerate(zip(sources, copies, strict=True))
+    ]
+    layer_body(shards, loads, *copies, *raws, out, *refs[2 * count + 7 :])
+
+
+def layer_body(
+    shards, loads, tokens, mix_pre, mix_post, mlp_pre, mlp_post, out_scale, down_scale,
     x_scale, gate_scale, up_scale, conv_weight, recur_map, input_map, decay_param,
     x_weight, gate_weight, out_weight, up_weight, down_weight, out,
     b_full, o_full, u_full, d_full, b_give, o_give, u_give, d_give,
     x_raw, gate_raw, o_raw, u_raw, d_raw, gains_full, gain_rows, scales, maps, rate,
-    tok_got, normed, branches, mixed, mlp_in, active, hidden,
+    tok_got, normed, branches, mixed, mlp_in, active, hidden, result,
     give, got_near, keep, total, stage, got_far,
     raw_sem, y_sent, y_land, z_sent, z_land, zf_sent, x_sent, x_land, g_sent, g_land,
-    t_sent, t_land, n_sent, n_land, f_sent, f_land, m_sent, m_land, mn_sent, mn_land, mf_sent, mf_land,
+    t_sent, t_land, n_sent, n_land, f_sent, f_land, m_sent, m_land, mn_sent, mn_land, mf_sent, mf_land, out_sem,
 ):
     lines = shards // 2
     others = lines - 1
@@ -403,10 +416,15 @@
     depth = z + upper * (lines - 1 - 2 * z)
     inner = (depth + lines - 1) // lines
 
+    def unfold(place):
+        return place + upper * (lines - 1 - 2 * place)
+
+    def early(k):
+        return 1 - (k + 2 * lines - 2 * depth) // (2 * lines)
+
     def other(k):
-        turned = lax.rem(k + inner * (others - 1), others)
-        place = turned + (turned + lines - depth) // lines
-        return place + upper * (lines - 1 - 2 * place)
+        near = depth + (1 - 2 * lax.rem(k, 2)) * (k // 2 + 1)
+        return unfold(k + 1 + early(k) * (near - k - 1))
 
     seq, width = tokens.shape
     share = seq // 2
@@ -423,12 +441,15 @@
         pltpu.make_async_copy(up_weight, u_raw, raw_sem.at[3]),
         pltpu.make_async_copy(down_weight, d_raw, raw_sem.at[4]),
     ]
-    for copy in raw_copies:
+    for copy in raw_copies[:2] + loads[1:] + raw_copies[2:] + loads[:1]:
         copy.start()
+    token_copy = loads[0]
     peers = [{"fs": lax.rem(me + step, shards)} for step in range(1, shards)] + [x_peer, core_peer]
     barrier = pltpu.get_barrier_semaphore()
     for peer in peers:
         pl.semaphore_signal(barrier, inc=1, device_id=peer, device_id_type=MESH_IDS)
+    for copy in loads[1:]:
+        copy.wait()
     for row, gain in enumerate((mix_pre, mix_post, mlp_pre, mlp_post)):
         gains_full[me, row : row + 1, :] = gain[...]
     chunk = 32
@@ -465,9 +486,10 @@
 
         return move
 
-    def half(w, slot, side):
+    def half(w, slot, side, cut):
         rows = gives[w].shape[0]
-        return fulls[w].at[pl.ds(aligned(slot * rows + side * (rows // 2), 64), rows // 2)]
+        size = rows // (2 * CUTS)
+        return fulls[w].at[pl.ds(aligned(slot * rows + (side * CUTS + cut) * size, 32), size)]
 
     def whole(w, slot):
         rows = gives[w].shape[0]
@@ -480,49 +502,53 @@
         block = whole(w, z * 2 + 1 - y)
         return push(block, block, y_sent.at[w], y_land.at[w], y_peer)
 
-    def z_copy(w, kind, k):
+    def z_copy(w, kind, way, cut):
         slot = z * 2 + lax.rem(y + kind, 2)
-        block = half(w, slot, rep)
-        return push(block, block, z_sent.at[w, kind, k], z_land.at[w, slot], {"fs": other(k) * 2 + y})
+        block = half(w, slot, rep, cut)
+        target = unfold(depth + 1 - 2 * way)
+        return push(block, block, z_sent.at[w, kind, way, cut], z_land.at[w, slot, cut], {"fs": target * 2 + y})
 
     def start_z(w, kind):
-        z_copy(w, kind, 1).start()
-        z_copy(w, kind, 0).start()
-        for k in range(2, others):
-
-            @pl.when((inner == 1) | (k < others - 1))
+        for cut in range(CUTS):
+
+            @pl.when(inner == 1)
             def _():
-                z_copy(w, kind, k).start()
+                z_copy(w, kind, 1, cut).start()
+
+            z_copy(w, kind, 0, cut).start()
 
     def item_slot(kind, k):
         return other(k) * 2 + lax.rem(y + kind, 2)
 
-    def zf_copy(w, kind):
-        slot = item_slot(kind, 0)
-        block = half(w, slot, rep)
-        return push(block, block, zf_sent.at[w, kind], z_land.at[w, slot], {"fs": upper * (lines - 1) * 2 + y})
-
-    def x_copy(w, kind, k):
+    def zf_copy(w, kind, k, cut):
         slot = item_slot(kind, k)
-        block = half(w, slot, rep)
-        return push(block, block, x_sent.at[w, kind, k], x_land.at[w, slot], x_peer)
+        block = half(w, slot, rep, cut)
+        target = unfold(depth - 1 + 2 * early(k) * lax.rem(k, 2))
+        return push(block, block, zf_sent.at[w, kind, k, cut], z_land.at[w, slot, cut], {"fs": target * 2 + y})
+
+    def x_copy(w, kind, k, cut):
+        slot = item_slot(kind, k)
+        block = half(w, slot, rep, cut)
+        return push(block, block, x_sent.at[w, kind, k, cut], x_land.at[w, slot, cut], x_peer)
 
     def serve(w, item):
         kind, k = item // others, lax.rem(item, others)
         slot = item_slot(kind, k)
-        block = half(w, slot, rep)
-        push(block, block, x_sent.at[w, kind, k], z_land.at[w, slot], x_peer).wait_recv()
-
-        @pl.when((k == 0) & (depth == 1))
-        def _():
-            zf_copy(w, kind).start()
-
-        x_copy(w, kind, k).start()
+        for cut in range(CUTS):
+            block = half(w, slot, rep, cut)
+            push(block, block, x_sent.at[w, kind, k, cut], z_land.at[w, slot, cut], x_peer).wait_recv()
+
+            @pl.when(inner == 1)
+            def _():
+                zf_copy(w, kind, k, cut).start()
+
+            x_copy(w, kind, k, cut).start()
 
     def x_arrival(w, item):
         slot = item_slot(item // others, lax.rem(item, others))
-        block = half(w, slot, 1 - rep)
-        push(block, block, x_sent.at[w, 0, 0], x_land.at[w, slot], x_peer).wait_recv()
+        for cut in range(CUTS):
+            block = half(w, slot, 1 - rep, cut)
+            push(block, block, x_sent.at[w, 0, 0, cut], x_land.at[w, slot, cut], x_peer).wait_recv()
 
     items = 2 * others
 
@@ -548,10 +574,10 @@
     raw_copies[1].wait()
     cast(b_give.shape[0], branch_rows)
     pl.semaphore_wait(barrier, len(peers))
+    for step in range(1, shards):
+        gain_copy(step).start()
     y_copy(0).start()
     start_z(0, 0)
-    for step in range(1, shards):
-        gain_copy(step).start()
     raw_copies[2].wait()
     cast(o_give.shape[0], column_rows(o_full, o_give, o_raw, out_scale))
     raw_copies[3].wait()
@@ -559,6 +585,7 @@
     raw_copies[4].wait()
     cast(d_give.shape[0], column_rows(d_full, d_give, d_raw, down_scale))
     y_copy(1).start()
+    token_copy.wait()
     t_near.start()
     y_copy(2).start()
     y_copy(3).start()
@@ -600,41 +627,70 @@
 
         lax.fori_loop(0, seq // rows, body, 0)
 
+    is_inner, is_end = inner == 1, inner == 0
+
+    def start_other(w):
+        y_arrival(w).wait_recv()
+        start_z(w, 1)
+
+    serve(0, 0)
+    serve(0, 1)
+    start_other(0)
+    when(is_end, lambda: start_z(1, 0))
     normalize(tokens, 0)
-    serve(0, 0)
-    y_arrival(0).wait_recv()
-    start_z(0, 1)
-    start_z(1, 0)
-    serve(0, 1)
     serve(0, 2)
-    y_arrival(1).wait_recv()
-    start_z(1, 1)
+
+    @pl.when(is_end)
+    def _():
+        start_other(1)
+        start_z(2, 0)
+
     serve(0, 3)
     serve(0, 4)
+    when(is_inner, lambda: start_z(1, 0))
     serve(0, 5)
-    t_near.wait_recv()
-    t_pass.start()
+    serve(1, 0)
+    serve(1, 1)
+
+    @pl.when(is_inner)
+    def _():
+        start_other(1)
+        start_z(2, 0)
+        serve(1, 2)
+        serve(1, 3)
+        serve(1, 4)
+
     all_x_arrivals(0)
 
     col_tiles = columns // PIECE
+
+    def pass_tokens():
+        t_near.wait_recv()
+        t_pass.start()
 
     def branch_step(index, carry):
         row = aligned((index // col_tiles) * seq, 64)
         col = aligned(lax.rem(index, col_tiles) * PIECE, PIECE)
         value = jnp.dot(normed[pl.ds(row, seq), :], b_full[:, pl.ds(col, PIECE)], preferred_element_type=F32)
         branches[pl.ds(row, seq), pl.ds(col, PIECE)] = (value * scales[:, pl.ds(col, PIECE)]).astype(BF16)
-        when(index >= 2, lambda: serve(1, index - 2))
+        when(index == 0, pass_tokens)
+        when(is_inner & (index == 1), lambda: serve(1, 5))
+
+        @pl.when(is_end & (lax.rem(index, 2) == 0))
+        def _():
+            serve(1, 2 + index // 2)
+
         return carry
 
     lax.fori_loop(0, col_tiles, branch_step, 0)
     t_pass.wait_recv()
     normalize(tok_got, seq)
+    when(is_end, lambda: start_other(2))
     lax.fori_loop(col_tiles, 2 * col_tiles, branch_step, 0)
-    start_z(2, 0)
-
-    def up_sends():
-        y_arrival(2).wait_recv()
-        start_z(2, 1)
+
+    def up_second():
+        serve(2, 1)
+        start_other(2)
 
     def mixer_step(index, carry):
         row = aligned((index // groups) * seq, 64)
@@ -647,17 +703,19 @@
             conv_weight[:, pl.ds(aligned(y * channels + col, LANES), LANES)],
             maps[pl.ds(aligned(group * 2 * LANES, LANES), 2 * LANES), :], rate[:, lanes],
         )
-        when(index == groups, up_sends)
-        when(index == 2 * groups - 2, lambda: serve(2, 0))
+        when(is_inner & (index == 3), lambda: serve(2, 0))
+        when(is_inner & (index == 4), up_second)
+        when(is_end & (index == 1), lambda: serve(2, 0))
+        when(is_end & (index == 5), lambda: serve(2, 1))
         return carry
 
     lax.fori_loop(0, 2 * groups, mixer_step, 0)
 
-    def block_of(index):
+    def block_of(index, flip=0):
         item = index - 2
         safe = lax.rem(item + items, items)
-        far = item_slot(safe // others, lax.rem(safe, others))
-        near = z * 2 + lax.rem(y + index, 2)
+        far = item_slot(safe // others + flip, lax.rem(safe, others))
+        near = z * 2 + lax.rem(y + index + flip, 2)
         late = (index + shards - 2) // shards
         return near + late * (far - near)
 
@@ -667,7 +725,7 @@
     def far_copy(phase, block):
         return push(stage.at[block], got_far.at[block], f_sent.at[phase, block], f_land.at[phase, block], y_peer)
 
-    def project(phase, w, lhs, before):
+    def project(phase, w, lhs, lag, before):
         depth_rows = gives[w].shape[0]
 
         def combine(index):
@@ -690,20 +748,25 @@
             own = lhs[pl.ds(aligned(seq + core * share, 64), share), :]
             keep[block] = jnp.dot(own, weight, preferred_element_type=F32)
             when(index > 0, lambda: combine(index - 1))
+            if lag < shards:
+                when(index >= lag, lambda: add_far(phase, index - lag))
             return carry
 
         lax.fori_loop(0, shards, body, 0)
         combine(shards - 1)
 
-    def collect(phase, between):
+    def add_far(phase, index):
+        block = block_of(index, 1)
+        far_copy(phase, block).wait_recv()
+        total[block] += got_far[block].astype(F32)
+
+    def collect(phase, lag, between):
         def body(index, carry):
-            block = block_of(index)
-            far_copy(phase, block).wait_recv()
-            total[block] += got_far[block].astype(F32)
+            add_far(phase, index)
             between(index)
             return carry
 
-        lax.fori_loop(0, shards, body, 0)
+        lax.fori_loop(shards - lag, shards, body, 0)
 
         def drain(index, carry):
             far_copy(phase, index).wait_send()
@@ -712,17 +775,26 @@
 
         lax.fori_loop(0, shards, drain, 0)
 
+    def during_project(index):
+        when(is_inner & (index == 3), lambda: serve(2, 2))
+        when(is_end & (index == 3), lambda: start_z(3, 0))
+
+    def last_up():
+        serve(2, 5)
+        start_z(3, 0)
+
     def during_sum(index):
-        when(index == 1, lambda: serve(2, 2))
-
-        @pl.when(index == 5)
-        def _():
-            serve(2, 3)
-            start_z(3, 0)
+        when(is_inner & (index == 0), lambda: serve(2, 3))
+        when(is_inner & (index == 1), lambda: serve(2, 4))
+        when(is_inner & (index == 4), last_up)
+        when(is_end & (index == 0), lambda: serve(2, 2))
+        when(is_end & (index == 1), lambda: serve(2, 3))
+        when(is_end & (index == 3), lambda: start_other(3))
+        when(is_end & (index == 4), lambda: serve(2, 4))
 
     all_x_arrivals(1)
-    project(0, 1, mixed, lambda index: when(index == 4, lambda: serve(2, 1)))
-    collect(0, during_sum)
+    project(0, 1, mixed, shards, during_project)
+    collect(0, shards, during_sum)
 
     def summed(start):
         values = [total[block, pl.ds(start, rows), :] for block in range(shards)]
@@ -776,10 +848,15 @@
         return carry
 
     lax.fori_loop(0, pieces, entry_piece, 0)
-    serve(2, 4)
-    y_arrival(3).wait_recv()
-    start_z(3, 1)
-    serve(2, 5)
+    when(is_end, lambda: serve(2, 5))
+    serve(3, 0)
+
+    @pl.when(is_inner)
+    def _():
+        serve(3, 1)
+        start_other(3)
+        serve(3, 2)
+
     all_x_arrivals(2)
 
     def wait_near(index, carry):
@@ -800,7 +877,6 @@
         lax.fori_loop(0, up_tiles, body, 0)
 
     up_rows(0)
-    serve(3, 0)
 
     def pass_on(index, carry):
         to_far(index).wait_recv()
@@ -808,7 +884,12 @@
         return carry
 
     lax.fori_loop(0, pieces, pass_on, 0)
-    serve(3, 1)
+    when(is_end, lambda: serve(3, 1))
+
+    @pl.when(is_inner)
+    def _():
+        serve(3, 3)
+        serve(3, 4)
 
     def wait_far(index, carry):
         onward(index).wait_recv()
@@ -818,36 +899,46 @@
     up_rows(seq)
 
     def before_down(index):
-        when((index >= 2) & (index < items), lambda: serve(3, index))
+        when(is_inner & (index == 0), lambda: serve(3, 5))
+        when(is_end & (index >= 2) & (index < items), lambda: serve(3, index))
         when(index >= 2, lambda: x_arrival(3, index - 2))
 
-    project(1, 3, active, before_down)
-    collect(1, lambda index: None)
-
-    def last_rows(index, carry):
-        start = aligned(index * rows, rows)
-        values, factor = summed(start)
-        for block in range(shards):
-            cols = pl.ds(block * piece_cols, piece_cols)
-            value = hidden[pl.ds(start, rows), cols].astype(F32) + values[block] * factor * gain_rows[3:4, cols]
-            out[pl.ds(start, rows), cols] = value.astype(BF16)
+    project(1, 3, active, 3, before_down)
+    collect(1, 3, lambda index: None)
+
+    def out_copy(index):
+        block = pl.ds(aligned(index * piece_rows, 16), piece_rows)
+        return pltpu.make_async_copy(result.at[block], out.at[block], out_sem.at[index])
+
+    def last_piece(index, carry):
+        def last_rows(inner_index, inner_carry):
+            start = aligned(index * piece_rows + inner_index * rows, rows)
+            values, factor = summed(start)
+            for block in range(shards):
+                cols = pl.ds(block * piece_cols, piece_cols)
+                value = hidden[pl.ds(start, rows), cols].astype(F32) + values[block] * factor * gain_rows[3:4, cols]
+                result[pl.ds(start, rows), cols] = value.astype(BF16)
+            return inner_carry
+
+        lax.fori_loop(0, piece_rows // rows, last_rows, 0)
+        out_copy(index).start()
         return carry
 
-    lax.fori_loop(0, share // rows, last_rows, 0)
+    lax.fori_loop(0, pieces, last_piece, 0)
 
     for w in range(WEIGHTS):
         y_copy(w).wait_send()
         for kind in range(2):
-            for k in range(others):
-                x_copy(w, kind, k).wait_send()
-
-                @pl.when((inner == 1) | (k < others - 1))
+            for cut in range(CUTS):
+                for k in range(others):
+                    x_copy(w, kind, k, cut).wait_send()
+                z_copy(w, kind, 0, cut).wait_send()
+
+                @pl.when(inner == 1)
                 def _():
-                    z_copy(w, kind, k).wait_send()
-
-            @pl.when(depth == 1)
-            def _():
-                zf_copy(w, kind).wait_send()
+                    z_copy(w, kind, 1, cut).wait_send()
+                    for k in range(others):
+                        zf_copy(w, kind, k, cut).wait_send()
 
     t_near.wait_send()
     t_pass.wait_send()
@@ -858,6 +949,7 @@
         to_far(index).wait_send()
         to_near(index).wait_send()
         onward(index).wait_send()
+        out_copy(index).wait()
         return carry
 
     lax.fori_loop(0, pieces, drain, 0)
@@ -874,7 +966,6 @@
     fan_in, channels, units = x_weight.shape[0], x_weight.shape[1] // 2, up_weight.shape[1] // 2
     piece_cols = width // shards
     dma = pltpu.SemaphoreType.DMA
-    vmem = pl.BlockSpec(memory_space=pltpu.VMEM)
     anywhere = pl.BlockSpec(memory_space=pl.ANY)
     part_shapes = ((fan_in, 2 * channels), (channels, piece_cols), (fan_in, units), (units, piece_cols))
     raws = (x_weight, gate_weight, out_weight, up_weight, down_weight)
@@ -884,12 +975,15 @@
             x_scale, gate_scale, up_scale,
         )
     ]
-    result = pl.pallas_call(
+    inputs = (tokens[0], *rows, conv_weight, recur_map.T, input_map.T, decay_param[None])
+    outcome = pl.pallas_call(
         functools.partial(layer_kernel, shards),
         out_shape=jax.ShapeDtypeStruct((share, width), BF16),
-        in_specs=[vmem] * 14 + [anywhere] * len(raws),
-        out_specs=vmem,
-        scratch_shapes=[pltpu.VMEM((shards * shape[0], shape[1]), BF16) for shape in part_shapes]
+        in_specs=[anywhere] * (len(inputs) + len(raws)),
+        out_specs=anywhere,
+        scratch_shapes=[pltpu.VMEM(value.shape, value.dtype) for value in inputs]
+        + [dma((len(inputs),))]
+        + [pltpu.VMEM((shards * shape[0], shape[1]), BF16) for shape in part_shapes]
         + [pltpu.VMEM(shape, BF16) for shape in part_shapes]
         + [pltpu.VMEM(raw.shape, F32) for raw in raws]
         + [
@@ -905,6 +999,7 @@
             pltpu.VMEM((2 * seq, width), BF16),
             pltpu.VMEM((2 * seq, units), BF16),
             pltpu.VMEM((share, width), BF16),
+            pltpu.VMEM((share, width), BF16),
             pltpu.VMEM((shards, 2, share, piece_cols), BF16),
             pltpu.VMEM((shards, 2, share, piece_cols), BF16),
             pltpu.VMEM((shards, share, piece_cols), F32),
@@ -912,20 +1007,20 @@
             pltpu.VMEM((shards, share, piece_cols), BF16),
             pltpu.VMEM((shards, share, piece_cols), BF16),
             dma((len(raws),)), dma((WEIGHTS,)), dma((WEIGHTS,)),
-            dma((WEIGHTS, 2, lines - 1)), dma((WEIGHTS, shards)), dma((WEIGHTS, 2)),
-            dma((WEIGHTS, 2, lines - 1)), dma((WEIGHTS, shards)),
+            dma((WEIGHTS, 2, 2, CUTS)), dma((WEIGHTS, shards, CUTS)), dma((WEIGHTS, 2, lines - 1, CUTS)),
+            dma((WEIGHTS, 2, lines - 1, CUTS)), dma((WEIGHTS, shards, CUTS)),
             dma((shards - 1,)), dma((shards,)),
             dma((2,)), dma((2,)),
             dma((2, shards)), dma((2, shards)), dma((2, shards)), dma((2, shards)),
-            dma((pieces,)), dma((pieces,)), dma((pieces,)), dma((pieces,)), dma((pieces,)), dma((pieces,)),
+            *[dma((pieces,))] * 7,
         ],
         compiler_params=pltpu.CompilerParams(
             collective_id=4, has_side_effects=True, vmem_limit_bytes=67_000_000
         ),
         cost_estimate=pl.CostEstimate(flops=20_000_000_000, bytes_accessed=80_000_000, transcendentals=0),
         name="layer",
-    )(tokens[0], *rows, conv_weight, recur_map.T, input_map.T, decay_param[None], *raws)
-    return result[None]
+    )(*inputs, *raws)
+    return outcome[None]
 
 
 def solution(mesh):

time: 228 us -> 197 us (0.86)
  Pallas kernels: 225 us -> 194 us
    pallas_call x1, Pallas kernels: 225 us -> 194 us  [on_device_paired(): pl.pallas_call(functools.partial(layer_kernel, shards), out_shape=jax.Sha...]
where the time goes in v3:
time: 197 us; the launch traced here: 196 us
  Pallas kernels  194 us (98%)
  local copies, waits for them, and re-layouts  2.3 us (1%)
    pallas_call x1, Pallas kernels, on_device_paired(): pl.pallas_call(functools.partial(layer_kernel, shards), out_shape=jax.Sha...  194 us

profile of v3, /device:TPU:0, one launch (start us, length us, event | category | flops | bytes accessed | tf_op | source)
XLA Modules:
  0.0 196.4 jit_solution(18446168996386683460)
XLA Ops:
  0.0 194.1 %layer.1 = bf16[256,2048]{1,0:T(8,128)(2,1)} custom-call(bf16[512,2048]{1,0:T(8,128)(2,1)} %bitcast.15, f32[1,256]{1,0:T(1,128)} %bitcast.22, f32[1,256]{1,0:T(1,128)} %bitcast.23, f32[1,256]{1,0:T(1,128)} %bitcast.24, f32[1,256]{1,0:T(1,128)} %bitcast.25, f32[1,256]{1,0:T(1,128)} %bitcast.26, f32[1,256]{1,0:T(1,128)} %bitcast.27, f32[1,1024]{1,0:T(1,128)} %bitcast.19, ...), custom_call_target="tpu_custom_call" | custom-call | flops 20000000000 | bytes 80000000 | tf_op jit(solution)/shard_map/layer/pallas_call | solution.py:979
  194.1 2.3 %copy.21 = bf16[1,256,2048]{2,1,0:T(8,128)(2,1)} copy(bf16[1,256,2048]{2,1,0:T(8,128)(2,1)} %bitcast.14) | data formatting | bytes 2097152

commit v4 on v3

--- a/solution.py
+++ b/solution.py
@@ -343,7 +343,7 @@
 
 WEIGHTS = 4
 PIECE = 256
-CUTS = 2
+CUTS = (2, 2, 2, 4)
 
 
 def log_decay_and_drive(conv, logits, rate):
@@ -488,8 +488,8 @@
 
     def half(w, slot, side, cut):
         rows = gives[w].shape[0]
-        size = rows // (2 * CUTS)
-        return fulls[w].at[pl.ds(aligned(slot * rows + (side * CUTS + cut) * size, 32), size)]
+        size = rows // (2 * CUTS[w])
+        return fulls[w].at[pl.ds(aligned(slot * rows + (side * CUTS[w] + cut) * size, 32), size)]
 
     def whole(w, slot):
         rows = gives[w].shape[0]
@@ -506,10 +506,10 @@
         slot = z * 2 + lax.rem(y + kind, 2)
         block = half(w, slot, rep, cut)
         target = unfold(depth + 1 - 2 * way)
-        return push(block, block, z_sent.at[w, kind, way, cut], z_land.at[w, slot, cut], {"fs": target * 2 + y})
+        return push(block, block, z_sent.at[w, way], z_land.at[w, slot, cut], {"fs": target * 2 + y})
 
     def start_z(w, kind):
-        for cut in range(CUTS):
+        for cut in range(CUTS[w]):
 
             @pl.when(inner == 1)
             def _():
@@ -524,19 +524,19 @@
         slot = item_slot(kind, k)
         block = half(w, slot, rep, cut)
         target = unfold(depth - 1 + 2 * early(k) * lax.rem(k, 2))
-        return push(block, block, zf_sent.at[w, kind, k, cut], z_land.at[w, slot, cut], {"fs": target * 2 + y})
+        return push(block, block, zf_sent.at[w], z_land.at[w, slot, cut], {"fs": target * 2 + y})
 
     def x_copy(w, kind, k, cut):
         slot = item_slot(kind, k)
         block = half(w, slot, rep, cut)
-        return push(block, block, x_sent.at[w, kind, k, cut], x_land.at[w, slot, cut], x_peer)
-
-    def serve(w, item):
+        return push(block, block, x_sent.at[w], x_land.at[w, slot], x_peer)
+
+    def serve(w, item, cuts=None):
         kind, k = item // others, lax.rem(item, others)
         slot = item_slot(kind, k)
-        for cut in range(CUTS):
+        for cut in range(CUTS[w]) if cuts is None else cuts:
             block = half(w, slot, rep, cut)
-            push(block, block, x_sent.at[w, kind, k, cut], z_land.at[w, slot, cut], x_peer).wait_recv()
+            push(block, block, x_sent.at[w], z_land.at[w, slot, cut], x_peer).wait_recv()
 
             @pl.when(inner == 1)
             def _():
@@ -546,9 +546,9 @@
 
     def x_arrival(w, item):
         slot = item_slot(item // others, lax.rem(item, others))
-        for cut in range(CUTS):
-            block = half(w, slot, 1 - rep, cut)
-            push(block, block, x_sent.at[w, 0, 0, cut], x_land.at[w, slot, cut], x_peer).wait_recv()
+        rows = gives[w].shape[0]
+        block = fulls[w].at[pl.ds(aligned(slot * rows + (1 - rep) * (rows // 2), 64), rows // 2)]
+        push(block, block, x_sent.at[w], x_land.at[w, slot], x_peer).wait_recv()
 
     items = 2 * others
 
@@ -568,7 +568,7 @@
 
     def gain_copy(step):
         block = gains_full.at[me]
-        return push(block, block, g_sent.at[step - 1], g_land.at[me], {"fs": lax.rem(me + step, shards)})
+        return push(block, block, g_sent, g_land.at[me], {"fs": lax.rem(me + step, shards)})
 
     raw_copies[0].wait()
     raw_copies[1].wait()
@@ -610,7 +610,7 @@
     for step in range(1, shards):
         source = lax.rem(me + step, shards)
         block = gains_full.at[source]
-        push(block, block, g_sent.at[step - 1], g_land.at[source], y_peer).wait_recv()
+        push(block, block, g_sent, g_land.at[source], y_peer).wait_recv()
     piece_cols = width // shards
     for block in range(shards):
         gain_rows[:, block * piece_cols : (block + 1) * piece_cols] = gains_full[block]
@@ -635,10 +635,11 @@
 
     serve(0, 0)
     serve(0, 1)
+    when(is_inner, lambda: serve(0, 2))
     start_other(0)
     when(is_end, lambda: start_z(1, 0))
     normalize(tokens, 0)
-    serve(0, 2)
+    when(is_end, lambda: serve(0, 2))
 
     @pl.when(is_end)
     def _():
@@ -647,15 +648,14 @@
 
     serve(0, 3)
     serve(0, 4)
+    serve(0, 5)
     when(is_inner, lambda: start_z(1, 0))
-    serve(0, 5)
     serve(1, 0)
     serve(1, 1)
 
     @pl.when(is_inner)
     def _():
         start_other(1)
-        start_z(2, 0)
         serve(1, 2)
         serve(1, 3)
         serve(1, 4)
@@ -663,6 +663,10 @@
     all_x_arrivals(0)
 
     col_tiles = columns // PIECE
+
+    def last_out():
+        serve(1, 5)
+        start_z(2, 0)
 
     def pass_tokens():
         t_near.wait_recv()
@@ -674,18 +678,24 @@
         value = jnp.dot(normed[pl.ds(row, seq), :], b_full[:, pl.ds(col, PIECE)], preferred_element_type=F32)
         branches[pl.ds(row, seq), pl.ds(col, PIECE)] = (value * scales[:, pl.ds(col, PIECE)]).astype(BF16)
         when(index == 0, pass_tokens)
-        when(is_inner & (index == 1), lambda: serve(1, 5))
-
-        @pl.when(is_end & (lax.rem(index, 2) == 0))
-        def _():
-            serve(1, 2 + index // 2)
+        when(is_inner & (index == 1), last_out)
+
+        when(is_end & (index == 0), lambda: serve(1, 3))
+        when(is_end & (index == 2), lambda: serve(1, 2))
+        when(is_end & (index == 6), lambda: serve(2, 0))
+        when(is_end & (index == 7), lambda: start_other(2))
 
         return carry
 
     lax.fori_loop(0, col_tiles, branch_step, 0)
     t_pass.wait_recv()
     normalize(tok_got, seq)
-    when(is_end, lambda: start_other(2))
+
+    @pl.when(is_end)
+    def _():
+        serve(1, 4)
+        serve(1, 5)
+
     lax.fori_loop(col_tiles, 2 * col_tiles, branch_step, 0)
 
     def up_second():
@@ -705,27 +715,31 @@
         )
         when(is_inner & (index == 3), lambda: serve(2, 0))
         when(is_inner & (index == 4), up_second)
-        when(is_end & (index == 1), lambda: serve(2, 0))
-        when(is_end & (index == 5), lambda: serve(2, 1))
+        when(is_end & (index == 2 * groups - 1), lambda: serve(2, 1))
         return carry
 
     lax.fori_loop(0, 2 * groups, mixer_step, 0)
+
+    def arrival(item):
+        gap = item - others + 1
+        swapped = 1 - (gap * (gap - 1) + 63) // 64
+        return item + swapped * (2 * others - 1 - 2 * item)
 
     def block_of(index, flip=0):
         item = index - 2
-        safe = lax.rem(item + items, items)
+        safe = arrival(lax.rem(item + items, items))
         far = item_slot(safe // others + flip, lax.rem(safe, others))
         near = z * 2 + lax.rem(y + index + flip, 2)
         late = (index + shards - 2) // shards
         return near + late * (far - near)
 
     def near_copy(phase, block):
-        return push(give.at[block], got_near.at[block], n_sent.at[phase, block], n_land.at[phase, block], core_peer)
+        return push(give.at[block], got_near.at[block], n_sent.at[phase], n_land.at[block], core_peer)
 
     def far_copy(phase, block):
-        return push(stage.at[block], got_far.at[block], f_sent.at[phase, block], f_land.at[phase, block], y_peer)
-
-    def project(phase, w, lhs, lag, before):
+        return push(stage.at[block], got_far.at[block], f_sent.at[phase], f_land.at[block], y_peer)
+
+    def project(phase, w, lhs, lag, before, after):
         depth_rows = gives[w].shape[0]
 
         def combine(index):
@@ -750,6 +764,7 @@
             when(index > 0, lambda: combine(index - 1))
             if lag < shards:
                 when(index >= lag, lambda: add_far(phase, index - lag))
+            after(index)
             return carry
 
         lax.fori_loop(0, shards, body, 0)
@@ -768,32 +783,28 @@
 
         lax.fori_loop(shards - lag, shards, body, 0)
 
-        def drain(index, carry):
-            far_copy(phase, index).wait_send()
-            near_copy(phase, index).wait_send()
-            return carry
-
-        lax.fori_loop(0, shards, drain, 0)
+        push(stage, stage, f_sent.at[phase], f_land.at[0], y_peer).wait_send()
+        push(give, give, n_sent.at[phase], n_land.at[0], core_peer).wait_send()
 
     def during_project(index):
-        when(is_inner & (index == 3), lambda: serve(2, 2))
-        when(is_end & (index == 3), lambda: start_z(3, 0))
+        when(is_inner & (index == 6), lambda: serve(2, 2))
+        when(is_end & (index == 0), lambda: start_z(3, 0))
+        when(is_end & (index == 6), lambda: serve(2, 3))
 
     def last_up():
         serve(2, 5)
         start_z(3, 0)
 
     def during_sum(index):
-        when(is_inner & (index == 0), lambda: serve(2, 3))
-        when(is_inner & (index == 1), lambda: serve(2, 4))
-        when(is_inner & (index == 4), last_up)
-        when(is_end & (index == 0), lambda: serve(2, 2))
-        when(is_end & (index == 1), lambda: serve(2, 3))
-        when(is_end & (index == 3), lambda: start_other(3))
-        when(is_end & (index == 4), lambda: serve(2, 4))
+        when(is_inner & (index == 1), lambda: serve(2, 3))
+        when(is_inner & (index == 2), lambda: serve(2, 4))
+        when(is_inner & (index == 5), last_up)
+        when(is_end & (index == 0), lambda: start_other(3))
+        when(is_end & (index == 1), lambda: serve(2, 2))
+        when(is_end & (index == 3), lambda: serve(2, 4))
 
     all_x_arrivals(1)
-    project(0, 1, mixed, shards, during_project)
+    project(0, 1, mixed, shards, during_project, lambda index: None)
     collect(0, shards, during_sum)
 
     def summed(start):
@@ -801,7 +812,7 @@
         squares = sum(jnp.sum(value * value, axis=-1, keepdims=True) for value in values)
         return values, lax.rsqrt(squares * (1.0 / width) + EPSILON)
 
-    pieces = m_sent.shape[0]
+    pieces = m_land.shape[0]
     piece_rows = share // pieces
 
     def piece(ref, base, index):
@@ -810,16 +821,16 @@
     def to_far(index):
         return push(
             piece(mlp_in, core * share, index), piece(mlp_in, seq + core * share, index),
-            m_sent.at[index], m_land.at[index], y_peer,
+            m_sent, m_land.at[index], y_peer,
         )
 
     def to_near(index):
         block = piece(mlp_in, core * share, index)
-        return push(block, block, mn_sent.at[index], mn_land.at[index], core_peer)
+        return push(block, block, mn_sent, mn_land.at[index], core_peer)
 
     def onward(index):
         block = piece(mlp_in, seq + core * share, index)
-        return push(block, block, mf_sent.at[index], mf_land.at[index], core_peer)
+        return push(block, block, mf_sent, mf_land.at[index], core_peer)
 
     def entry_piece(index, carry):
         def entry_rows(inner_index, inner_carry):
@@ -847,8 +858,9 @@
         to_near(index).start()
         return carry
 
+    when(is_end, lambda: serve(2, 5, (0,)))
     lax.fori_loop(0, pieces, entry_piece, 0)
-    when(is_end, lambda: serve(2, 5))
+    when(is_end, lambda: serve(2, 5, range(1, CUTS[2])))
     serve(3, 0)
 
     @pl.when(is_inner)
@@ -877,6 +889,7 @@
         lax.fori_loop(0, up_tiles, body, 0)
 
     up_rows(0)
+    when(is_end, lambda: serve(3, 1))
 
     def pass_on(index, carry):
         to_far(index).wait_recv()
@@ -884,7 +897,7 @@
         return carry
 
     lax.fori_loop(0, pieces, pass_on, 0)
-    when(is_end, lambda: serve(3, 1))
+    when(is_end, lambda: serve(3, 3, (0, 1)))
 
     @pl.when(is_inner)
     def _():
@@ -900,10 +913,13 @@
 
     def before_down(index):
         when(is_inner & (index == 0), lambda: serve(3, 5))
-        when(is_end & (index >= 2) & (index < items), lambda: serve(3, index))
-        when(index >= 2, lambda: x_arrival(3, index - 2))
-
-    project(1, 3, active, 3, before_down)
+        when(index >= 2, lambda: x_arrival(3, arrival(index - 2)))
+
+    def after_down(index):
+        when(is_end & (index >= 2) & (index < items - 1), lambda: serve(3, arrival(index + 1)))
+
+    when(is_end, lambda: serve(3, 3, range(2, CUTS[3])))
+    project(1, 3, active, 3, before_down, after_down)
     collect(1, 3, lambda index: None)
 
     def out_copy(index):
@@ -928,31 +944,29 @@
 
     for w in range(WEIGHTS):
         y_copy(w).wait_send()
-        for kind in range(2):
-            for cut in range(CUTS):
-                for k in range(others):
-                    x_copy(w, kind, k, cut).wait_send()
-                z_copy(w, kind, 0, cut).wait_send()
-
-                @pl.when(inner == 1)
-                def _():
-                    z_copy(w, kind, 1, cut).wait_send()
-                    for k in range(others):
-                        zf_copy(w, kind, k, cut).wait_send()
+        sent = fulls[w].at[pl.ds(0, others * gives[w].shape[0])]
+        own = fulls[w].at[pl.ds(0, gives[w].shape[0])]
+        push(sent, sent, x_sent.at[w], x_land.at[w, 0], x_peer).wait_send()
+        push(own, own, z_sent.at[w, 0], x_land.at[w, 0], x_peer).wait_send()
+
+        @pl.when(inner == 1)
+        def _():
+            push(own, own, z_sent.at[w, 1], x_land.at[w, 0], x_peer).wait_send()
+            push(sent, sent, zf_sent.at[w], x_land.at[w, 0], x_peer).wait_send()
 
     t_near.wait_send()
     t_pass.wait_send()
-    for step in range(1, shards):
-        gain_copy(step).wait_send()
+    most = gains_full.at[pl.ds(0, shards - 1)]
+    push(most, most, g_sent, g_land.at[0], y_peer).wait_send()
 
     def drain(index, carry):
-        to_far(index).wait_send()
-        to_near(index).wait_send()
-        onward(index).wait_send()
         out_copy(index).wait()
         return carry
 
     lax.fori_loop(0, pieces, drain, 0)
+    block = mlp_in.at[pl.ds(0, share)]
+    for sent in (m_sent, mn_sent, mf_sent):
+        push(block, block, sent, m_land.at[0], y_peer).wait_send()
 
 
 def on_device_paired(
@@ -1007,12 +1021,12 @@
             pltpu.VMEM((shards, share, piece_cols), BF16),
             pltpu.VMEM((shards, share, piece_cols), BF16),
             dma((len(raws),)), dma((WEIGHTS,)), dma((WEIGHTS,)),
-            dma((WEIGHTS, 2, 2, CUTS)), dma((WEIGHTS, shards, CUTS)), dma((WEIGHTS, 2, lines - 1, CUTS)),
-            dma((WEIGHTS, 2, lines - 1, CUTS)), dma((WEIGHTS, shards, CUTS)),
-            dma((shards - 1,)), dma((shards,)),
+            dma((WEIGHTS, 2)), dma((WEIGHTS, shards, max(CUTS))), dma((WEIGHTS,)),
+            dma((WEIGHTS,)), dma((WEIGHTS, shards)),
+            dma, dma((shards,)),
             dma((2,)), dma((2,)),
-            dma((2, shards)), dma((2, shards)), dma((2, shards)), dma((2, shards)),
-            *[dma((pieces,))] * 7,
+            dma((2,)), dma((shards,)), dma((2,)), dma((shards,)),
+            dma, dma((pieces,)), dma, dma((pieces,)), dma, dma((pieces,)), dma((pieces,)),
         ],
         compiler_params=pltpu.CompilerParams(
             collective_id=4, has_side_effects=True, vmem_limit_bytes=67_000_000

time: 197 us -> 187 us (0.949)
  Pallas kernels: 194 us -> 184 us
    pallas_call x1, Pallas kernels: 194 us -> 184 us  [on_device_paired(): pl.pallas_call(functools.partial(layer_kernel, shards), out_shape=jax.Sha...]
where the time goes in v4:
time: 187 us
  Pallas kernels  184 us (98%)
  local copies, waits for them, and re-layouts  2.3 us (1%)
    pallas_call x1, Pallas kernels, on_device_paired(): pl.pallas_call(functools.partial(layer_kernel, shards), out_shape=jax.Sha...  184 us

profile of v4, /device:TPU:0, one launch (start us, length us, event | category | flops | bytes accessed | tf_op | source)
XLA Modules:
  0.0 186.7 jit_solution(2614938732191151760)
XLA Ops:
  0.0 184.4 %layer.1 = bf16[256,2048]{1,0:T(8,128)(2,1)} custom-call(bf16[512,2048]{1,0:T(8,128)(2,1)} %bitcast.15, f32[1,256]{1,0:T(1,128)} %bitcast.22, f32[1,256]{1,0:T(1,128)} %bitcast.23, f32[1,256]{1,0:T(1,128)} %bitcast.24, f32[1,256]{1,0:T(1,128)} %bitcast.25, f32[1,256]{1,0:T(1,128)} %bitcast.26, f32[1,256]{1,0:T(1,128)} %bitcast.27, f32[1,1024]{1,0:T(1,128)} %bitcast.19, ...), custom_call_target="tpu_custom_call" | custom-call | flops 20000000000 | bytes 80000000 | tf_op jit(solution)/shard_map/layer/pallas_call | solution.py:993
  184.4 2.3 %copy.21 = bf16[1,256,2048]{2,1,0:T(8,128)(2,1)} copy(bf16[1,256,2048]{2,1,0:T(8,128)(2,1)} %bitcast.14) | data formatting | bytes 2097152

commit v5 on v4

--- a/solution.py
+++ b/solution.py
@@ -343,7 +343,7 @@
 
 WEIGHTS = 4
 PIECE = 256
-CUTS = (2, 2, 2, 4)
+CUTS = (2, 1, 4, 4)
 
 
 def log_decay_and_drive(conv, logits, rate):
@@ -384,27 +384,45 @@
     return pl.multiple_of(start, unit)
 
 
+def arrival_item(item, others):
+    gap = item - others + 1
+    swapped = 1 - (gap * (gap - 1) + 63) // 64
+    return item + swapped * (2 * others - 1 - 2 * item)
+
+
+def far_lag(shards):
+    others = shards // 2 - 1
+
+    def place(index):
+        if index < 2:
+            return 1 - index
+        kind, k = divmod(arrival_item(index - 2, others), others)
+        return arrival_item((1 - kind) * others + k, others) + 2
+
+    return next(lag for lag in range(1, shards + 1) if all(place(i) < i + lag for i in range(shards - lag)))
+
+
 def layer_kernel(shards, *refs):
     count = 14
-    sources, raws, out = refs[:count], refs[count : count + 5], refs[count + 5]
-    copies = refs[count + 6 : 2 * count + 6]
-    load_sem = refs[2 * count + 6]
+    sources, raws, outs = refs[:count], refs[count : count + 5], refs[count + 5 : count + 9]
+    copies = refs[count + 9 : 2 * count + 9]
+    load_sem = refs[2 * count + 9]
     loads = [
         pltpu.make_async_copy(source, copy, load_sem.at[at])
         for at, (source, copy) in enumerate(zip(sources, copies, strict=True))
     ]
-    layer_body(shards, loads, *copies, *raws, out, *refs[2 * count + 7 :])
+    layer_body(shards, loads, *copies, *raws, *outs, *refs[2 * count + 10 :])
 
 
 def layer_body(
     shards, loads, tokens, mix_pre, mix_post, mlp_pre, mlp_post, out_scale, down_scale,
     x_scale, gate_scale, up_scale, conv_weight, recur_map, input_map, decay_param,
-    x_weight, gate_weight, out_weight, up_weight, down_weight, out,
+    x_weight, gate_weight, out_weight, up_weight, down_weight, out_total, out_factor, out_hidden, out_gain,
     b_full, o_full, u_full, d_full, b_give, o_give, u_give, d_give,
     x_raw, gate_raw, o_raw, u_raw, d_raw, gains_full, gain_rows, scales, maps, rate,
-    tok_got, normed, branches, mixed, mlp_in, active, hidden, result,
+    tok_got, normed, branches, mixed, mlp_in, active, hidden, lane_squares,
     give, got_near, keep, total, stage, got_far,
-    raw_sem, y_sent, y_land, z_sent, z_land, zf_sent, x_sent, x_land, g_sent, g_land,
+    raw_sem, y_sent, y_land, z_sent, b_land, o_land, u_land, d_land, zf_sent, x_sent, x_land, g_sent, g_land,
     t_sent, t_land, n_sent, n_land, f_sent, f_land, m_sent, m_land, mn_sent, mn_land, mf_sent, mf_land, out_sem,
 ):
     lines = shards // 2
@@ -433,6 +451,7 @@
     units = active.shape[1]
     gives = (b_give, o_give, u_give, d_give)
     fulls = (b_full, o_full, u_full, d_full)
+    z_land = (b_land, o_land, u_land, d_land)
 
     raw_copies = [
         pltpu.make_async_copy(x_weight, x_raw, raw_sem.at[0]),
@@ -506,7 +525,7 @@
         slot = z * 2 + lax.rem(y + kind, 2)
         block = half(w, slot, rep, cut)
         target = unfold(depth + 1 - 2 * way)
-        return push(block, block, z_sent.at[w, way], z_land.at[w, slot, cut], {"fs": target * 2 + y})
+        return push(block, block, z_sent.at[w, way], z_land[w].at[slot, cut], {"fs": target * 2 + y})
 
     def start_z(w, kind):
         for cut in range(CUTS[w]):
@@ -524,7 +543,7 @@
         slot = item_slot(kind, k)
         block = half(w, slot, rep, cut)
         target = unfold(depth - 1 + 2 * early(k) * lax.rem(k, 2))
-        return push(block, block, zf_sent.at[w], z_land.at[w, slot, cut], {"fs": target * 2 + y})
+        return push(block, block, zf_sent.at[w], z_land[w].at[slot, cut], {"fs": target * 2 + y})
 
     def x_copy(w, kind, k, cut):
         slot = item_slot(kind, k)
@@ -536,7 +555,7 @@
         slot = item_slot(kind, k)
         for cut in range(CUTS[w]) if cuts is None else cuts:
             block = half(w, slot, rep, cut)
-            push(block, block, x_sent.at[w], z_land.at[w, slot, cut], x_peer).wait_recv()
+            push(block, block, x_sent.at[w], z_land[w].at[slot, cut], x_peer).wait_recv()
 
             @pl.when(inner == 1)
             def _():
@@ -615,6 +634,8 @@
     for block in range(shards):
         gain_rows[:, block * piece_cols : (block + 1) * piece_cols] = gains_full[block]
 
+    gain_out = pltpu.make_async_copy(gain_rows.at[pl.ds(3, 1)], out_gain, out_sem.at[shards + 1])
+    gain_out.start()
     rows = 16
 
     def normalize(source, base):
@@ -715,15 +736,13 @@
         )
         when(is_inner & (index == 3), lambda: serve(2, 0))
         when(is_inner & (index == 4), up_second)
-        when(is_end & (index == 2 * groups - 1), lambda: serve(2, 1))
+        when(is_end & (lax.rem(index, 2) == 1), lambda: serve(2, 1, (index // 2,)))
         return carry
 
     lax.fori_loop(0, 2 * groups, mixer_step, 0)
 
     def arrival(item):
-        gap = item - others + 1
-        swapped = 1 - (gap * (gap - 1) + 63) // 64
-        return item + swapped * (2 * others - 1 - 2 * item)
+        return arrival_item(item, others)
 
     def block_of(index, flip=0):
         item = index - 2
@@ -739,6 +758,10 @@
     def far_copy(phase, block):
         return push(stage.at[block], got_far.at[block], f_sent.at[phase], f_land.at[block], y_peer)
 
+    def out_copy(block):
+        cols = pl.ds(aligned(block * piece_cols, LANES), piece_cols)
+        return pltpu.make_async_copy(total.at[block], out_total.at[:, cols], out_sem.at[block])
+
     def project(phase, w, lhs, lag, before, after):
         depth_rows = gives[w].shape[0]
 
@@ -750,6 +773,8 @@
             far_copy(phase, block).start()
 
         def body(index, carry):
+            if phase == 1:
+                when(index > 0, lambda: combine(index - 1))
             before(index)
             block = block_of(index)
             weight = fulls[w][pl.ds(aligned(block * depth_rows, 64), depth_rows), :]
@@ -761,7 +786,8 @@
             near_copy(phase, block).start()
             own = lhs[pl.ds(aligned(seq + core * share, 64), share), :]
             keep[block] = jnp.dot(own, weight, preferred_element_type=F32)
-            when(index > 0, lambda: combine(index - 1))
+            if phase == 0:
+                when(index > 0, lambda: combine(index - 1))
             if lag < shards:
                 when(index >= lag, lambda: add_far(phase, index - lag))
             after(index)
@@ -773,7 +799,13 @@
     def add_far(phase, index):
         block = block_of(index, 1)
         far_copy(phase, block).wait_recv()
-        total[block] += got_far[block].astype(F32)
+        value = total[block] + got_far[block].astype(F32)
+        total[block] = value
+        if phase == 1:
+            lane_squares[...] += sum(
+                jnp.square(value[:, at : at + LANES]) for at in range(0, piece_cols, LANES)
+            )
+            out_copy(block).start()
 
     def collect(phase, lag, between):
         def body(index, carry):
@@ -789,7 +821,7 @@
     def during_project(index):
         when(is_inner & (index == 6), lambda: serve(2, 2))
         when(is_end & (index == 0), lambda: start_z(3, 0))
-        when(is_end & (index == 6), lambda: serve(2, 3))
+        when(is_end & (lax.rem(index, 2) == 1), lambda: serve(2, 3, (index // 2,)))
 
     def last_up():
         serve(2, 5)
@@ -800,8 +832,9 @@
         when(is_inner & (index == 2), lambda: serve(2, 4))
         when(is_inner & (index == 5), last_up)
         when(is_end & (index == 0), lambda: start_other(3))
-        when(is_end & (index == 1), lambda: serve(2, 2))
-        when(is_end & (index == 3), lambda: serve(2, 4))
+        when(is_end & (index >= 1) & (index < 5), lambda: serve(2, 2, (index - 1,)))
+        when(is_end & (index == 5), lambda: serve(2, 4, (0, 1)))
+        when(is_end & (index >= 6), lambda: serve(2, 4, (index - 4,)))
 
     all_x_arrivals(1)
     project(0, 1, mixed, shards, during_project, lambda index: None)
@@ -860,6 +893,9 @@
 
     when(is_end, lambda: serve(2, 5, (0,)))
     lax.fori_loop(0, pieces, entry_piece, 0)
+    hidden_out = pltpu.make_async_copy(hidden, out_hidden, out_sem.at[shards + 2])
+    hidden_out.start()
+    lane_squares[...] = jnp.zeros_like(lane_squares)
     when(is_end, lambda: serve(2, 5, range(1, CUTS[2])))
     serve(3, 0)
 
@@ -916,31 +952,19 @@
         when(index >= 2, lambda: x_arrival(3, arrival(index - 2)))
 
     def after_down(index):
-        when(is_end & (index >= 2) & (index < items - 1), lambda: serve(3, arrival(index + 1)))
+        when(is_end & (index >= 2) & (index < items - 2), lambda: serve(3, arrival(index + 1)))
+        when(is_end & (index == items - 1), lambda: serve(3, items - 1, (0, 1)))
+        when(is_end & (index == items), lambda: serve(3, items - 1, range(2, CUTS[3])))
 
     when(is_end, lambda: serve(3, 3, range(2, CUTS[3])))
-    project(1, 3, active, 3, before_down, after_down)
-    collect(1, 3, lambda index: None)
-
-    def out_copy(index):
-        block = pl.ds(aligned(index * piece_rows, 16), piece_rows)
-        return pltpu.make_async_copy(result.at[block], out.at[block], out_sem.at[index])
-
-    def last_piece(index, carry):
-        def last_rows(inner_index, inner_carry):
-            start = aligned(index * piece_rows + inner_index * rows, rows)
-            values, factor = summed(start)
-            for block in range(shards):
-                cols = pl.ds(block * piece_cols, piece_cols)
-                value = hidden[pl.ds(start, rows), cols].astype(F32) + values[block] * factor * gain_rows[3:4, cols]
-                result[pl.ds(start, rows), cols] = value.astype(BF16)
-            return inner_carry
-
-        lax.fori_loop(0, piece_rows // rows, last_rows, 0)
-        out_copy(index).start()
-        return carry
-
-    lax.fori_loop(0, pieces, last_piece, 0)
+    lag = far_lag(shards)
+    project(1, 3, active, lag, before_down, after_down)
+    collect(1, lag, lambda index: None)
+
+    squares = jnp.sum(lane_squares[...], axis=-1, keepdims=True)
+    lane_squares[...] = jnp.broadcast_to(lax.rsqrt(squares * (1.0 / width) + EPSILON), lane_squares.shape)
+    factor_copy = pltpu.make_async_copy(lane_squares, out_factor, out_sem.at[shards])
+    factor_copy.start()
 
     for w in range(WEIGHTS):
         y_copy(w).wait_send()
@@ -959,14 +983,45 @@
     most = gains_full.at[pl.ds(0, shards - 1)]
     push(most, most, g_sent, g_land.at[0], y_peer).wait_send()
 
+    block = mlp_in.at[pl.ds(0, share)]
+    for sent in (m_sent, mn_sent, mf_sent):
+        push(block, block, sent, m_land.at[0], y_peer).wait_send()
+
     def drain(index, carry):
         out_copy(index).wait()
         return carry
 
-    lax.fori_loop(0, pieces, drain, 0)
-    block = mlp_in.at[pl.ds(0, share)]
-    for sent in (m_sent, mn_sent, mf_sent):
-        push(block, block, sent, m_land.at[0], y_peer).wait_send()
+    lax.fori_loop(0, shards, drain, 0)
+    gain_out.wait()
+    hidden_out.wait()
+    factor_copy.wait()
+
+
+def finish_kernel(total, factor, hidden, gain, out, total_in, factor_in, hidden_in, gain_in, result, row_sem, sem, out_sem):
+    pieces = out_sem.shape[0]
+    size = total.shape[0] // pieces
+    near = [pltpu.make_async_copy(factor, factor_in, row_sem.at[0]), pltpu.make_async_copy(gain, gain_in, row_sem.at[1])]
+    loads, stores = [], []
+    for index in range(pieces):
+        block = pl.ds(index * size, size)
+        loads.append([
+            pltpu.make_async_copy(total.at[block], total_in.at[block], sem.at[0, index]),
+            pltpu.make_async_copy(hidden.at[block], hidden_in.at[block], sem.at[1, index]),
+        ])
+        stores.append(pltpu.make_async_copy(result.at[block], out.at[block], out_sem.at[index]))
+    for copy in near + sum(loads, []):
+        copy.start()
+    for copy in near:
+        copy.wait()
+    for index in range(pieces):
+        block = pl.ds(index * size, size)
+        for copy in loads[index]:
+            copy.wait()
+        scaled = total_in[block, :] * factor_in[block, :1] * gain_in[...]
+        result[block, :] = (hidden_in[block, :].astype(F32) + scaled).astype(BF16)
+        stores[index].start()
+    for copy in stores:
+        copy.wait()
 
 
 def on_device_paired(
@@ -990,11 +1045,16 @@
         )
     ]
     inputs = (tokens[0], *rows, conv_weight, recur_map.T, input_map.T, decay_param[None])
-    outcome = pl.pallas_call(
+    total, factor, hidden, gain = pl.pallas_call(
         functools.partial(layer_kernel, shards),
-        out_shape=jax.ShapeDtypeStruct((share, width), BF16),
+        out_shape=(
+            jax.ShapeDtypeStruct((share, width), F32),
+            jax.ShapeDtypeStruct((share, LANES), F32),
+            jax.ShapeDtypeStruct((share, width), BF16),
+            jax.ShapeDtypeStruct((1, width), F32),
+        ),
         in_specs=[anywhere] * (len(inputs) + len(raws)),
-        out_specs=anywhere,
+        out_specs=(anywhere,) * 4,
         scratch_shapes=[pltpu.VMEM(value.shape, value.dtype) for value in inputs]
         + [dma((len(inputs),))]
         + [pltpu.VMEM((shards * shape[0], shape[1]), BF16) for shape in part_shapes]
@@ -1013,7 +1073,7 @@
             pltpu.VMEM((2 * seq, width), BF16),
             pltpu.VMEM((2 * seq, units), BF16),
             pltpu.VMEM((share, width), BF16),
-            pltpu.VMEM((share, width), BF16),
+            pltpu.VMEM((share, LANES), F32),
             pltpu.VMEM((shards, 2, share, piece_cols), BF16),
             pltpu.VMEM((shards, 2, share, piece_cols), BF16),
             pltpu.VMEM((shards, share, piece_cols), F32),
@@ -1021,12 +1081,12 @@
             pltpu.VMEM((shards, share, piece_cols), BF16),
             pltpu.VMEM((shards, share, piece_cols), BF16),
             dma((len(raws),)), dma((WEIGHTS,)), dma((WEIGHTS,)),
-            dma((WEIGHTS, 2)), dma((WEIGHTS, shards, max(CUTS))), dma((WEIGHTS,)),
+            dma((WEIGHTS, 2)), *[dma((shards, cuts)) for cuts in CUTS], dma((WEIGHTS,)),
             dma((WEIGHTS,)), dma((WEIGHTS, shards)),
             dma, dma((shards,)),
             dma((2,)), dma((2,)),
             dma((2,)), dma((shards,)), dma((2,)), dma((shards,)),
-            dma, dma((pieces,)), dma, dma((pieces,)), dma, dma((pieces,)), dma((pieces,)),
+            dma, dma((pieces,)), dma, dma((pieces,)), dma, dma((pieces,)), dma((shards + 3,)),
         ],
         compiler_params=pltpu.CompilerParams(
             collective_id=4, has_side_effects=True, vmem_limit_bytes=67_000_000
@@ -1034,7 +1094,16 @@
         cost_estimate=pl.CostEstimate(flops=20_000_000_000, bytes_accessed=80_000_000, transcendentals=0),
         name="layer",
     )(*inputs, *raws)
-    return outcome[None]
+    finals = (total, factor, hidden, gain)
+    return pl.pallas_call(
+        finish_kernel,
+        in_specs=[anywhere] * len(finals),
+        out_specs=anywhere,
+        out_shape=jax.ShapeDtypeStruct((share, width), BF16),
+        scratch_shapes=[pltpu.VMEM(value.shape, value.dtype) for value in finals]
+        + [pltpu.VMEM((share, width), BF16), dma((2,)), dma((2, pieces)), dma((pieces,))],
+        name="finish",
+    )(*finals)[None]
 
 
 def solution(mesh):
@@ -1051,7 +1120,7 @@
     out_specs = P(("rep", "fs"), "tp", None)
     paired = (
         mesh.shape["rep"] == 2 and mesh.shape["tp"] == 2
-        and mesh.shape["fs"] % 4 == 0 and mesh.shape["fs"] > 4
+        and mesh.shape["fs"] % 4 == 0 and 4 < mesh.shape["fs"] < 16
     )
     return jax.shard_map(
         on_device_paired if paired else on_device, mesh=mesh, in_specs=in_specs, out_specs=out_specs, check_vma=False

time: 187 us -> 182 us (0.973)
  local copies, waits for them, and re-layouts: 2.3 us -> 0 us
  Pallas kernels: 184 us -> 182 us
    pallas_call x1 -> x2, Pallas kernels: 184 us -> 182 us  [the longest x1 179 us: on_device_paired(): pl.pallas_call(functools.partial(layer_kernel, shards), out_shape=(jax.Sh...]
    unnamed x1 -> x0, local copies, waits for them, and re-layouts: 2.3 us -> none
where the time goes in v5:
time: 182 us
  Pallas kernels  182 us (100%)
    pallas_call x1, Pallas kernels, on_device_paired(): pl.pallas_call(functools.partial(layer_kernel, shards), out_shape=(jax.Sh...  179 us

profile of v5, /device:TPU:0, one launch (start us, length us, event | category | flops | bytes accessed | tf_op | source)
XLA Modules:
  0.0 181.8 jit_solution(1295702082413482134)
XLA Ops:
  0.0 178.8 %layer.1 = (f32[256,2048]{1,0:T(8,128)}, f32[256,128]{1,0:T(8,128)}, bf16[256,2048]{1,0:T(8,128)(2,1)}, f32[1,2048]{1,0:T(1,128)}) custom-call(bf16[512,2048]{1,0:T(8,128)(2,1)} %bitcast.14, f32[1,256]{1,0:T(1,128)} %bitcast.21, f32[1,256]{1,0:T(1,128)} %bitcast.22, f32[1,256]{1,0:T(1,128)} %bitcast.23, f32[1,256]{1,0:T(1,128)} %bitcast.24, ...), custom_call_target="tpu_custom_call" | custom-call | flops 20000000000 | bytes 80000000 | tf_op jit(solution)/shard_map/layer/pallas_call | solution.py:1048
  178.8 3.0 %finish.1 = bf16[256,2048]{1,0:T(8,128)(2,1)} custom-call(f32[256,2048]{1,0:T(8,128)} %get-tuple-element.9.total, f32[256,128]{1,0:T(8,128)} %get-tuple-element.10.factor, bf16[256,2048]{1,0:T(8,128)(2,1)} %get-tuple-element.11.hidden, f32[1,2048]{1,0:T(1,128)} %get-tuple-element.12.gain), custom_call_target="tpu_custom_call" | custom-call | tf_op jit(solution)/shard_map/finish/pallas_call | solution.py:1098

commit v6 on v5

--- a/solution.py
+++ b/solution.py
@@ -343,7 +343,7 @@
 
 WEIGHTS = 4
 PIECE = 256
-CUTS = (2, 1, 4, 4)
+CUTS = (4, 1, 4, 4)
 
 
 def log_decay_and_drive(conv, logits, rate):
@@ -545,10 +545,13 @@
         target = unfold(depth - 1 + 2 * early(k) * lax.rem(k, 2))
         return push(block, block, zf_sent.at[w], z_land[w].at[slot, cut], {"fs": target * 2 + y})
 
+    def x_sem(w, slot):
+        return x_land.at[w + slot if w == WEIGHTS - 1 else w]
+
     def x_copy(w, kind, k, cut):
         slot = item_slot(kind, k)
         block = half(w, slot, rep, cut)
-        return push(block, block, x_sent.at[w], x_land.at[w, slot], x_peer)
+        return push(block, block, x_sent.at[w], x_sem(w, slot), x_peer)
 
     def serve(w, item, cuts=None):
         kind, k = item // others, lax.rem(item, others)
@@ -567,16 +570,13 @@
         slot = item_slot(item // others, lax.rem(item, others))
         rows = gives[w].shape[0]
         block = fulls[w].at[pl.ds(aligned(slot * rows + (1 - rep) * (rows // 2), 64), rows // 2)]
-        push(block, block, x_sent.at[w], x_land.at[w, slot], x_peer).wait_recv()
+        push(block, block, x_sent.at[w], x_sem(w, slot), x_peer).wait_recv()
 
     items = 2 * others
 
     def all_x_arrivals(w):
-        def body(index, carry):
-            x_arrival(w, index)
-            return carry
-
-        lax.fori_loop(0, items, body, 0)
+        block = fulls[w].at[pl.ds(0, others * gives[w].shape[0])]
+        push(block, block, x_sent.at[w], x_land.at[w], x_peer).wait_recv()
 
     def when(condition, act):
         pl.when(condition)(act)
@@ -587,7 +587,7 @@
 
     def gain_copy(step):
         block = gains_full.at[me]
-        return push(block, block, g_sent, g_land.at[me], {"fs": lax.rem(me + step, shards)})
+        return push(block, block, g_sent, g_land, {"fs": lax.rem(me + step, shards)})
 
     raw_copies[0].wait()
     raw_copies[1].wait()
@@ -626,10 +626,8 @@
             first = (group * 2 + at) * LANES
             maps[first : first + LANES, :] = jnp.where(same, spread, 0.0).astype(BF16)
 
-    for step in range(1, shards):
-        source = lax.rem(me + step, shards)
-        block = gains_full.at[source]
-        push(block, block, g_sent, g_land.at[source], y_peer).wait_recv()
+    most = gains_full.at[pl.ds(0, shards - 1)]
+    push(most, most, g_sent, g_land, y_peer).wait_recv()
     piece_cols = width // shards
     for block in range(shards):
         gain_rows[:, block * piece_cols : (block + 1) * piece_cols] = gains_full[block]
@@ -638,7 +636,7 @@
     gain_out.start()
     rows = 16
 
-    def normalize(source, base):
+    def normalize(source, base, first, last):
         def body(index, carry):
             start = aligned(index * rows, rows)
             values = source[pl.ds(start, rows), :].astype(F32)
@@ -646,7 +644,7 @@
             normed[pl.ds(aligned(base + start, rows), rows), :] = values.astype(BF16)
             return carry
 
-        lax.fori_loop(0, seq // rows, body, 0)
+        lax.fori_loop(first // rows, last // rows, body, 0)
 
     is_inner, is_end = inner == 1, inner == 0
 
@@ -659,7 +657,7 @@
     when(is_inner, lambda: serve(0, 2))
     start_other(0)
     when(is_end, lambda: start_z(1, 0))
-    normalize(tokens, 0)
+    normalize(tokens, 0, 0, seq)
     when(is_end, lambda: serve(0, 2))
 
     @pl.when(is_end)
@@ -710,12 +708,10 @@
 
     lax.fori_loop(0, col_tiles, branch_step, 0)
     t_pass.wait_recv()
-    normalize(tok_got, seq)
-
-    @pl.when(is_end)
-    def _():
-        serve(1, 4)
-        serve(1, 5)
+    normalize(tok_got, seq, 0, share)
+    when(is_end, lambda: serve(1, 4))
+    normalize(tok_got, seq, share, seq)
+    when(is_end, lambda: serve(1, 5))
 
     lax.fori_loop(col_tiles, 2 * col_tiles, branch_step, 0)
 
@@ -752,8 +748,10 @@
         late = (index + shards - 2) // shards
         return near + late * (far - near)
 
-    def near_copy(phase, block):
-        return push(give.at[block], got_near.at[block], n_sent.at[phase], n_land.at[block], core_peer)
+    def near_copy(phase, block, side):
+        return push(
+            give.at[block, side], got_near.at[block, side], n_sent.at[phase], n_land.at[block, side], core_peer
+        )
 
     def far_copy(phase, block):
         return push(stage.at[block], got_far.at[block], f_sent.at[phase], f_land.at[block], y_peer)
@@ -767,10 +765,11 @@
 
         def combine(index):
             block = block_of(index)
-            near_copy(phase, block).wait_recv()
+            near_copy(phase, block, 1).wait_recv()
             stage[block] = (keep[block] + got_near[block, 1].astype(F32)).astype(BF16)
+            far_copy(phase, block).start()
+            near_copy(phase, block, 0).wait_recv()
             total[block] += got_near[block, 0].astype(F32)
-            far_copy(phase, block).start()
 
         def body(index, carry):
             if phase == 1:
@@ -778,14 +777,12 @@
             before(index)
             block = block_of(index)
             weight = fulls[w][pl.ds(aligned(block * depth_rows, 64), depth_rows), :]
-            for side in range(2):
+            for side, held in ((1, keep), (0, total)):
                 left = lhs[pl.ds(aligned(side * seq + (1 - core) * share, 64), share), :]
                 give[block, side] = jnp.dot(left, weight, preferred_element_type=F32).astype(BF16)
-            own = lhs[pl.ds(aligned(core * share, 64), share), :]
-            total[block] = jnp.dot(own, weight, preferred_element_type=F32)
-            near_copy(phase, block).start()
-            own = lhs[pl.ds(aligned(seq + core * share, 64), share), :]
-            keep[block] = jnp.dot(own, weight, preferred_element_type=F32)
+                left = lhs[pl.ds(aligned(side * seq + core * share, 64), share), :]
+                held[block] = jnp.dot(left, weight, preferred_element_type=F32)
+                near_copy(phase, block, side).start()
             if phase == 0:
                 when(index > 0, lambda: combine(index - 1))
             if lag < shards:
@@ -816,7 +813,7 @@
         lax.fori_loop(shards - lag, shards, body, 0)
 
         push(stage, stage, f_sent.at[phase], f_land.at[0], y_peer).wait_send()
-        push(give, give, n_sent.at[phase], n_land.at[0], core_peer).wait_send()
+        push(give, give, n_sent.at[phase], n_land.at[0, 0], core_peer).wait_send()
 
     def during_project(index):
         when(is_inner & (index == 6), lambda: serve(2, 2))
@@ -859,11 +856,11 @@
 
     def to_near(index):
         block = piece(mlp_in, core * share, index)
-        return push(block, block, mn_sent, mn_land.at[index], core_peer)
+        return push(block, block, mn_sent, mn_land, core_peer)
 
     def onward(index):
         block = piece(mlp_in, seq + core * share, index)
-        return push(block, block, mf_sent, mf_land.at[index], core_peer)
+        return push(block, block, mf_sent, mf_land, core_peer)
 
     def entry_piece(index, carry):
         def entry_rows(inner_index, inner_carry):
@@ -907,25 +904,23 @@
 
     all_x_arrivals(2)
 
-    def wait_near(index, carry):
-        to_near(index).wait_recv()
-        return carry
-
-    lax.fori_loop(0, pieces, wait_near, 0)
+    peer_rows = mlp_in.at[pl.ds(0, share)]
+    push(peer_rows, peer_rows, mn_sent, mn_land, core_peer).wait_recv()
     up_tiles = units // PIECE
 
-    def up_rows(base):
+    def up_rows(base, item):
         def body(index, carry):
             col = aligned(index * PIECE, PIECE)
             value = jnp.dot(mlp_in[pl.ds(base, seq), :], u_full[:, pl.ds(col, PIECE)], preferred_element_type=F32)
             value = jnp.maximum(value * up_scale[:, pl.ds(aligned(y * units + col, PIECE), PIECE)], 0.0)
             active[pl.ds(base, seq), pl.ds(col, PIECE)] = (value * value).astype(BF16)
+            when(is_end & (index == 2), lambda: serve(3, item, (item - 1,)))
             return carry
 
         lax.fori_loop(0, up_tiles, body, 0)
 
-    up_rows(0)
-    when(is_end, lambda: serve(3, 1))
+    up_rows(0, 1)
+    when(is_end, lambda: serve(3, 1, range(1, CUTS[3])))
 
     def pass_on(index, carry):
         to_far(index).wait_recv()
@@ -940,23 +935,21 @@
         serve(3, 3)
         serve(3, 4)
 
-    def wait_far(index, carry):
-        onward(index).wait_recv()
-        return carry
-
-    lax.fori_loop(0, pieces, wait_far, 0)
-    up_rows(seq)
+    push(peer_rows, peer_rows, mf_sent, mf_land, core_peer).wait_recv()
+    up_rows(seq, 3)
 
     def before_down(index):
         when(is_inner & (index == 0), lambda: serve(3, 5))
         when(index >= 2, lambda: x_arrival(3, arrival(index - 2)))
 
     def after_down(index):
-        when(is_end & (index >= 2) & (index < items - 2), lambda: serve(3, arrival(index + 1)))
+        when(is_end & (index < 2), lambda: serve(3, arrival(3), (index,)))
+        when(is_end & (index == 2), lambda: serve(3, arrival(3), range(2, CUTS[3])))
+        when(is_end & (index > 2) & (index < items - 2), lambda: serve(3, arrival(index + 1)))
         when(is_end & (index == items - 1), lambda: serve(3, items - 1, (0, 1)))
         when(is_end & (index == items), lambda: serve(3, items - 1, range(2, CUTS[3])))
 
-    when(is_end, lambda: serve(3, 3, range(2, CUTS[3])))
+    when(is_end, lambda: serve(3, 3, range(3, CUTS[3])))
     lag = far_lag(shards)
     project(1, 3, active, lag, before_down, after_down)
     collect(1, lag, lambda index: None)
@@ -970,18 +963,17 @@
         y_copy(w).wait_send()
         sent = fulls[w].at[pl.ds(0, others * gives[w].shape[0])]
         own = fulls[w].at[pl.ds(0, gives[w].shape[0])]
-        push(sent, sent, x_sent.at[w], x_land.at[w, 0], x_peer).wait_send()
-        push(own, own, z_sent.at[w, 0], x_land.at[w, 0], x_peer).wait_send()
+        push(sent, sent, x_sent.at[w], x_land.at[w], x_peer).wait_send()
+        push(own, own, z_sent.at[w, 0], x_land.at[w], x_peer).wait_send()
 
         @pl.when(inner == 1)
         def _():
-            push(own, own, z_sent.at[w, 1], x_land.at[w, 0], x_peer).wait_send()
-            push(sent, sent, zf_sent.at[w], x_land.at[w, 0], x_peer).wait_send()
+            push(own, own, z_sent.at[w, 1], x_land.at[w], x_peer).wait_send()
+            push(sent, sent, zf_sent.at[w], x_land.at[w], x_peer).wait_send()
 
     t_near.wait_send()
     t_pass.wait_send()
-    most = gains_full.at[pl.ds(0, shards - 1)]
-    push(most, most, g_sent, g_land.at[0], y_peer).wait_send()
+    push(most, most, g_sent, g_land, y_peer).wait_send()
 
     block = mlp_in.at[pl.ds(0, share)]
     for sent in (m_sent, mn_sent, mf_sent):
@@ -1082,11 +1074,11 @@
             pltpu.VMEM((shards, share, piece_cols), BF16),
             dma((len(raws),)), dma((WEIGHTS,)), dma((WEIGHTS,)),
             dma((WEIGHTS, 2)), *[dma((shards, cuts)) for cuts in CUTS], dma((WEIGHTS,)),
-            dma((WEIGHTS,)), dma((WEIGHTS, shards)),
-            dma, dma((shards,)),
+            dma((WEIGHTS,)), dma((WEIGHTS - 1 + shards,)),
+            dma, dma,
             dma((2,)), dma((2,)),
-            dma((2,)), dma((shards,)), dma((2,)), dma((shards,)),
-            dma, dma((pieces,)), dma, dma((pieces,)), dma, dma((pieces,)), dma((shards + 3,)),
+            dma((2,)), dma((shards, 2)), dma((2,)), dma((shards,)),
+            dma, dma((pieces,)), dma, dma, dma, dma, dma((shards + 3,)),
         ],
         compiler_params=pltpu.CompilerParams(
             collective_id=4, has_side_effects=True, vmem_limit_bytes=67_000_000

time: 182 us -> 180 us (0.989)
  Pallas kernels: 182 us -> 179 us
    pallas_call x1, Pallas kernels: 179 us -> 177 us  [on_device_paired(): pl.pallas_call(functools.partial(layer_kernel, shards), out_shape=(jax.Sh...]
where the time goes in v6:
time: 180 us
  Pallas kernels  179 us (99%)
    pallas_call x1, Pallas kernels, on_device_paired(): pl.pallas_call(functools.partial(layer_kernel, shards), out_shape=(jax.Sh...  177 us

profile of v6, /device:TPU:0, one launch (start us, length us, event | category | flops | bytes accessed | tf_op | source)
XLA Modules:
  0.0 179.5 jit_solution(9118454349606393561)
XLA Ops:
  0.0 176.5 %layer.1 = (f32[256,2048]{1,0:T(8,128)}, f32[256,128]{1,0:T(8,128)}, bf16[256,2048]{1,0:T(8,128)(2,1)}, f32[1,2048]{1,0:T(1,128)}) custom-call(bf16[512,2048]{1,0:T(8,128)(2,1)} %bitcast.14, f32[1,256]{1,0:T(1,128)} %bitcast.21, f32[1,256]{1,0:T(1,128)} %bitcast.22, f32[1,256]{1,0:T(1,128)} %bitcast.23, f32[1,256]{1,0:T(1,128)} %bitcast.24, ...), custom_call_target="tpu_custom_call" | custom-call | flops 20000000000 | bytes 80000000 | tf_op jit(solution)/shard_map/layer/pallas_call | solution.py:1040
  176.5 3.0 %finish.1 = bf16[256,2048]{1,0:T(8,128)(2,1)} custom-call(f32[256,2048]{1,0:T(8,128)} %get-tuple-element.9.total, f32[256,128]{1,0:T(8,128)} %get-tuple-element.10.factor, bf16[256,2048]{1,0:T(8,128)(2,1)} %get-tuple-element.11.hidden, f32[1,2048]{1,0:T(1,128)} %get-tuple-element.12.gain), custom_call_target="tpu_custom_call" | custom-call | tf_op jit(solution)/shard_map/finish/pallas_call | solution.py:1090
